TPU v7x, 32 devices: a whole 2x2x4 slice. The times are simulated.
32 devices in a mesh: ep: 8 (over z, x), tp: 4 (over y, core).
Axes of the slice: x: 2, y: 2, z: 4, core: 2. Of those that a mesh axis runs over, the one named last changes fastest.
Arguments:
- queries: bfloat16 [2048, 1536], P('ep', 'tp'), may hold values from -600 to 600
- compressed_key_value: bfloat16 [2048, 512], P('ep'), may hold values from -6 to 6
- rope_key: bfloat16 [2048, 32], P('ep'), may hold values from -6 to 6
- latent_norm_gain: float32 [512], replicated, may hold values from 0.1 to 1.9
- latent_to_key_value: bfloat16 [512, 2048], P(None, 'tp'), may hold values from -0.25 to 0.25
- out_proj: bfloat16 [1024, 2048], P(None, 'tp'), may hold values from -1.5 to 1.5
- moe_input: bfloat16 [2048, 2048], P('ep'), may hold values from -6 to 6
- moe_gain: float32 [2048], replicated, may hold values from 0.1 to 1.9
- routes: int32 [2048, 2], P('ep'), may hold values from 0 to 7, all different within a row; in each aligned block of 256 rows (0 to 255, 256 to 511, ...) at most 96 rows name the same one
- route_weight: float32 [2048, 2], P('ep'), may hold values from 0.2 to 1
- gate_weight: bfloat16 [8, 2048, 4096], P('ep', None, 'tp'), may hold values from -0.125 to 0.125
- up_weight: bfloat16 [8, 2048, 4096], P('ep', None, 'tp'), may hold values from -0.125 to 0.125
- down_weight: bfloat16 [8, 4096, 2048], P('ep', 'tp'), may hold values from -0.09375 to 0.09375
Outputs:
- attention_out: bfloat16 [2048, 2048], P('ep', 'tp')
- expert_out: bfloat16 [2048, 2048], P('ep', 'tp')
Inputs may be any that keep to these rules, and one draw needn't show every extreme that they name: `routes`: each row names 2 different experts. In the rows of one device (aligned blocks of 256 rows) no expert is named by more than 96 rows, and in some blocks one expert is named by exactly 96 rows.
All inputs are finite; a program needn't handle non-finite values.
Results may differ from a plain program's by a relative error of at most 0.019.
The roundings to bfloat16 on the way count: a program that leaves them out, or rounds other values in their place, can miss the bound.
Values may be sent and summed in bfloat16 or wider, within the bound.
A program may use at most 128 MiB of HBM per device.

v0:
```python
import functools

import jax
import jax.numpy as jnp
from jax import lax
from jax.experimental import pallas as pl
from jax.experimental.pallas import tpu as pltpu
from jax.sharding import PartitionSpec as P

PLAIN_HEAD_DIM = 64
ROPE = 32
VALUE_HEAD_DIM = 64
LANES = 128
CORES = 2
RELAY_GROUPS = 4
CHUNKS = 2


EPSILON = 1e-06
ROPE_BASE_VALUE = 10000.0


def rms_scale(values, gain_vector):
    floats = values.astype(jnp.float32)
    return (
        floats
        * lax.rsqrt(jnp.mean(floats * floats, axis=-1, keepdims=True) + EPSILON)
        * gain_vector
    )


def rotary(values, positions):
    full_width = values.shape[-1]
    half_dim = full_width // 2
    frequency = ROPE_BASE_VALUE ** (-jnp.arange(half_dim, dtype=jnp.float32) * 2.0 / full_width)
    angles = positions[..., None] * frequency
    cosine = jnp.cos(angles)
    sine_part = jnp.sin(angles)
    first_half = values[..., :half_dim]
    second_half = values[..., half_dim:]
    return jnp.concatenate(
        [
            first_half * cosine - second_half * sine_part,
            second_half * cosine + first_half * sine_part,
        ],
        axis=-1,
    )


def ep_shape(n_ep):
    nx = 2 if n_ep % 2 == 0 else 1
    nz = n_ep // nx
    order = [0] if nz == 1 else [0, nz // 2] + [d for d in range(1, nz) if d != nz // 2]
    return nx, nz, order


def merge_rows(block):
    return block.reshape(block.shape[0] * block.shape[1], block.shape[2])


def fused(
    n_ep,
    n_tp,
    heads,
    scale,
    q_ref,
    lat_ref,
    wkv_ref,
    wo_ref,
    moe_ref,
    wg_hbm,
    wu_hbm,
    wd_hbm,
    att_out,
    back,
    wg,
    wu,
    wd,
    g_lat,
    g_moe,
    g_att,
    kv,
    hidden,
    part,
    r1,
    s2,
    r2,
    tot,
    wsem,
    loc_sem,
    lat_a,
    lat_x,
    lat_c,
    moe_a,
    moe_y,
    moe_c,
    att_y,
    att_c,
    red_c,
    red_y,
    ret_a,
):
    me = lax.axis_index("ep")
    tp = lax.axis_index("tp")
    n_y = n_tp // CORES
    my_y = tp // CORES
    my_c = lax.rem(tp, CORES)
    mate = my_y * CORES + (1 - my_c)
    groups = min(RELAY_GROUPS, n_ep)
    per = n_ep // groups
    nx, nz, order = ep_shape(n_ep)
    my_z = me // nx
    my_x = lax.rem(me, nx)
    sends = []

    def ahead(s):
        z = lax.rem(my_z + order[s // nx], nz)
        return z * nx + lax.rem(my_x + s % nx, nx)

    def behind(s):
        z = lax.rem(my_z + nz - order[s // nx], nz)
        return z * nx + lax.rem(my_x + nx - s % nx, nx)

    def to(src, dst, sems, index, ep_id, tp_id):
        copy = pltpu.make_async_remote_copy(
            src_ref=src,
            dst_ref=dst,
            send_sem=sems.at[(0,) + index],
            recv_sem=sems.at[(1,) + index],
            device_id=(ep_id, tp_id),
            device_id_type=pl.DeviceIdType.MESH,
        )
        copy.start()
        sends.append(copy)
        return copy

    barrier = pltpu.get_barrier_semaphore()
    for d in range(1, n_ep):
        pl.semaphore_signal(
            barrier,
            inc=1,
            device_id=(lax.rem(me + d, n_ep), tp),
            device_id_type=pl.DeviceIdType.MESH,
        )
    for d in range(1, n_tp):
        pl.semaphore_signal(
            barrier,
            inc=1,
            device_id=(me, lax.rem(tp + d, n_tp)),
            device_id_type=pl.DeviceIdType.MESH,
        )
    pl.semaphore_wait(barrier, n_ep + n_tp - 2)

    moe_in = [pltpu.make_async_copy(moe_ref.at[me], g_moe.at[tp, 0], loc_sem.at[1])]
    moe_in[0].start()
    for s in range(1, n_ep):
        moe_in.append(to(moe_ref.at[ahead(s)], g_moe.at[tp, s], moe_a, (s,), ahead(s), tp))
    own_lat = my_c * nx
    lat_in = [pltpu.make_async_copy(lat_ref, g_lat.at[own_lat, 0], loc_sem.at[0])]
    lat_in[0].start()
    for i in range(1, nz):
        lat_in.append(
            to(lat_ref, g_lat.at[own_lat, i], lat_a, (i,), ahead(i * nx), tp)
        )
    lat_over = []

    def lat_relay(steps):
        for i in steps:
            if i == 0:
                lat_in[0].wait()
            else:
                lat_in[i].wait_recv()
            mine = g_lat.at[own_lat, i]
            lat_over.append(to(mine, mine, lat_c, (0, i), me, mate))
            if nx > 1:
                side = g_lat.at[own_lat + 1, i]
                lat_side.append(to(mine, side, lat_x, (i,), my_z * nx + 1 - my_x, tp))

    lat_side = []

    def lat_last():
        for i, copy in enumerate(lat_side):
            copy.wait_recv()
            side = g_lat.at[own_lat + 1, i]
            lat_over.append(to(side, side, lat_c, (1, i), me, mate))
        for copy in lat_over:
            copy.wait_recv()

    weights = []
    for i, (source, target) in enumerate(((wg_hbm, wg), (wu_hbm, wu), (wd_hbm, wd))):
        copy = pltpu.make_async_copy(source, target, wsem.at[i])
        copy.start()
        weights.append(copy)

    class Relay:
        def __init__(self, copies, buffer, ysem, csem):
            self.copies, self.buffer, self.ysem, self.csem = copies, buffer, ysem, csem
            self.y, self.c = {}, {}

        def view(self, t, g):
            return self.buffer.at[t, pl.ds(g * per, per)]

        def spread(self, g):
            for d in range(g * per, (g + 1) * per):
                if d == 0:
                    self.copies[0].wait()
                else:
                    self.copies[d].wait_recv()
            self.y[g] = []
            for o in range(1, n_y):
                other = lax.rem(my_y + o, n_y) * CORES + my_c
                self.y[g].append(
                    to(self.view(tp, g), self.view(tp, g), self.ysem, (o, g), me, other)
                )
            self.c[g] = [to(self.view(tp, g), self.view(tp, g), self.csem, (0, g), me, mate)]

        def forward(self, g):
            for o in range(1, n_y):
                self.y[g][o - 1].wait_recv()
                came = lax.rem(my_y + n_y - o, n_y) * CORES + my_c
                self.c[g].append(
                    to(self.view(came, g), self.view(came, g), self.csem, (o, g), me, mate)
                )

        def finish(self, g):
            for copy in self.c[g]:
                copy.wait_recv()

    moe = Relay(moe_in, g_moe, moe_y, moe_c)
    block = nz * lat_ref.shape[0]
    latent = wkv_ref.shape[0]

    def expand(t, carry):
        rows = merge_rows(g_lat[t])
        kv[pl.ds(pl.multiple_of(t * block, block), block), :] = jnp.dot(
            rows[:, :latent], wkv_ref[...], preferred_element_type=jnp.float32
        ).astype(jnp.bfloat16)
        return carry

    whole_lat = g_lat.reshape(g_lat.shape[0] * block, g_lat.shape[3])
    lane = lax.broadcasted_iota(jnp.int32, (1, LANES), 1)
    packed = 2 if heads % 2 == 0 else 1
    att_in, att_mate = [], []

    def attend(part_index):
        for h in range(part_index * packed, (part_index + 1) * packed):
            head = kv[:, h * LANES : (h + 1) * LANES]
            keys = jnp.where(lane < PLAIN_HEAD_DIM, head, whole_lat[:, latent : latent + LANES])
            scores = (
                lax.dot_general(
                    q_ref[:, h * LANES : (h + 1) * LANES],
                    keys,
                    (((1,), (1,)), ((), ())),
                    preferred_element_type=jnp.float32,
                )
                * scale
            )
            top = jnp.max(scores, axis=-1, keepdims=True)
            e = jnp.exp(scores - top)
            total = jnp.sum(e, axis=-1, keepdims=True)
            mixed = (
                jnp.dot(e.astype(jnp.bfloat16), head, preferred_element_type=jnp.float32) / total
            )
            if packed == 1:
                mixed = jnp.where(lane < PLAIN_HEAD_DIM, 0.0, mixed)
            elif h % 2 == 0:
                held = pltpu.roll(mixed, VALUE_HEAD_DIM, 1)
            else:
                mixed = jnp.where(lane < VALUE_HEAD_DIM, held, mixed)
        g_att[tp, part_index] = mixed.astype(jnp.bfloat16)

    def att_send(p):
        own = g_att.at[tp, p]
        for o in range(1, n_y):
            other = lax.rem(my_y + o, n_y) * CORES + my_c
            att_in.append((p, o, to(own, own, att_y, (o, p), me, other)))
        att_mate.append(to(own, own, att_c, (0, p), me, mate))

    slots = n_ep // CHUNKS
    cap = moe_ref.shape[1]
    rows = slots * cap
    columns = moe_ref.shape[2]
    ff = wg.shape[1]
    tile = min(256, ff)

    def up(c):
        for g in range(groups):
            if (g * per) // slots == c:
                moe.finish(g)

        def one(f, carry):
            span = pl.ds(pl.multiple_of(f * tile, tile), tile)
            gate = jnp.zeros((rows, tile), jnp.float32)
            lift = jnp.zeros((rows, tile), jnp.float32)
            for t in range(n_tp):
                x = merge_rows(g_moe[t, c * slots : (c + 1) * slots])
                gate += jnp.dot(
                    x, wg[t * columns : (t + 1) * columns, span], preferred_element_type=jnp.float32
                )
                lift += jnp.dot(
                    x, wu[t * columns : (t + 1) * columns, span], preferred_element_type=jnp.float32
                )
            hidden[:, span] = (gate / (1.0 + jnp.exp(-gate)) * lift).astype(jnp.bfloat16)
            return carry

        lax.fori_loop(0, ff // tile, one, 0)

    def down(c):
        def one(t, carry):
            span = pl.ds(pl.multiple_of(t * columns, columns), columns)
            part[t, c * slots : (c + 1) * slots] = (
                jnp.dot(hidden[...], wd[:, span], preferred_element_type=jnp.float32)
                .astype(jnp.bfloat16)
                .reshape(slots, cap, columns)
            )
            return carry

        lax.fori_loop(0, n_tp, one, 0)

    reduce_c, reduce_y = {}, {}

    def swap(c):
        span = pl.ds(c * slots, slots)
        for o in list(range(1, n_y)) + [0]:
            y = lax.rem(my_y + o, n_y)
            reduce_c[c, o] = to(
                part.at[y * CORES + (1 - my_c), span], r1.at[o, span], red_c, (o, c), me, mate
            )

    def level_two(c):
        span = pl.ds(c * slots, slots)
        for o in range(1, n_y):
            y = lax.rem(my_y + o, n_y)
            reduce_c[c, o].wait_recv()
            s2[o, span] = (
                part[y * CORES + my_c, span].astype(jnp.float32) + r1[o, span].astype(jnp.float32)
            ).astype(jnp.bfloat16)
            reduce_y[c, o] = to(
                s2.at[o, span], r2.at[o, span], red_y, (o, c), me, y * CORES + my_c
            )

    returns = []

    def give_back(c):
        span = pl.ds(c * slots, slots)
        reduce_c[c, 0].wait_recv()
        total = part[tp, span].astype(jnp.float32) + r1[0, span].astype(jnp.float32)
        for o in range(1, n_y):
            reduce_y[c, o].wait_recv()
            total += r2[o, span].astype(jnp.float32)
        tot[span] = total.astype(jnp.bfloat16)
        for d in range(c * slots, (c + 1) * slots):
            if d == 0:
                back[0] = tot[0]
            else:
                returns.append(to(tot.at[d], back.at[d], ret_a, (d,), behind(d), tp))

    def att_forward():
        for p, o, copy in att_in:
            copy.wait_recv()
            came = g_att.at[lax.rem(my_y + n_y - o, n_y) * CORES + my_c, p]
            att_mate.append(to(came, came, att_c, (o, p), me, mate))

    def project():
        for copy in att_mate:
            copy.wait_recv()
        total = jnp.zeros(att_out.shape, jnp.float32)
        for t in range(n_tp):
            x = jnp.concatenate([g_att[t, p] for p in range(g_att.shape[1])], axis=1)
            width = x.shape[1]
            total += jnp.dot(
                x, wo_ref[t * width : (t + 1) * width, :], preferred_element_type=jnp.float32
            )
        att_out[...] = total.astype(jnp.bfloat16)

    parts = heads // packed
    half = groups // 2
    for g in range(half):
        moe.spread(g)
        if g > 0:
            moe.forward(g - 1)
    moe.forward(half - 1)
    moe.spread(half)
    for copy in weights:
        copy.wait()
    up(0)
    moe.forward(half)
    for g in range(half + 1, groups):
        moe.spread(g)
        moe.forward(g)
    down(0)
    swap(0)
    lat_relay(range(0, nz // 2))
    up(1)
    level_two(0)
    down(1)
    swap(1)
    lat_relay(range(nz // 2, nz))
    give_back(0)
    level_two(1)
    lat_last()
    lax.fori_loop(0, g_lat.shape[0], expand, 0)
    for p in range(parts):
        attend(p)
        if p == 0:
            give_back(1)
        att_send(p)
    att_forward()
    project()
    for copy in returns:
        copy.wait_recv()
    for copy in sends:
        copy.wait_send()


def local(
    queries,
    compressed_key_value,
    rope_key,
    latent_norm_gain,
    latent_to_key_value,
    out_proj,
    moe_input,
    moe_gain,
    routes,
    route_weight,
    gate_weight,
    up_weight,
    down_weight,
):
    n_ep = lax.axis_size("ep")
    n_tp = lax.axis_size("tp")
    me = lax.axis_index("ep")
    tp = lax.axis_index("tp")
    n_y = n_tp // CORES
    bf16 = jnp.bfloat16
    row_count = queries.shape[0]
    heads = latent_to_key_value.shape[1] // (PLAIN_HEAD_DIM + VALUE_HEAD_DIM)
    latent = compressed_key_value.shape[1]
    positions = (me * row_count + jnp.arange(row_count, dtype=jnp.int32)).astype(jnp.float32)
    q_heads = queries.reshape(row_count, heads, PLAIN_HEAD_DIM + ROPE)
    q_rope = rotary(q_heads[..., PLAIN_HEAD_DIM:].astype(jnp.float32), positions[:, None])
    pad = LANES - PLAIN_HEAD_DIM - ROPE
    q_all = jnp.concatenate(
        [
            q_heads[..., :PLAIN_HEAD_DIM],
            q_rope.astype(bf16),
            jnp.zeros((row_count, heads, pad), bf16),
        ],
        axis=-1,
    ).reshape(row_count, heads * LANES)
    share = row_count // CORES
    nx, nz, order = ep_shape(n_ep)
    cut = lambda x: lax.dynamic_slice_in_dim(x, lax.rem(tp, CORES) * share, share, 0)
    lat = jnp.concatenate(
        [
            rms_scale(cut(compressed_key_value), latent_norm_gain).astype(bf16),
            jnp.zeros((share, PLAIN_HEAD_DIM), bf16),
            rotary(cut(rope_key).astype(jnp.float32), cut(positions)).astype(bf16),
            jnp.zeros((share, pad), bf16),
        ],
        axis=1,
    )
    if heads % 2 == 0:
        wo = out_proj
        parts = heads // 2
    else:
        wo = out_proj.reshape(n_tp * heads, VALUE_HEAD_DIM, out_proj.shape[1])
        wo = jnp.concatenate([jnp.zeros_like(wo), wo], axis=1)
        wo = wo.reshape(n_tp * heads * LANES, out_proj.shape[1])
        parts = heads

    moe_rows, model_width = moe_input.shape
    top = routes.shape[1]
    capacity = 3 * moe_rows // n_ep
    places = -(-capacity // 16) * 16
    columns = model_width // n_tp
    flat = routes.reshape(-1)
    hot = (flat[:, None] == jnp.arange(n_ep, dtype=jnp.int32)[None, :]).astype(bf16)
    pairs = flat.shape[0]
    before = jnp.tril(jnp.ones((pairs, pairs), bf16), -1)
    earlier = jnp.dot(before, hot, preferred_element_type=jnp.float32)
    slot = jnp.sum(earlier * hot.astype(jnp.float32), axis=1).astype(jnp.int32)
    destination = (flat * places + slot).reshape(moe_rows, top)
    normed = rms_scale(moe_input, moe_gain).astype(bf16)
    own_normed = lax.dynamic_slice_in_dim(normed, tp * columns, columns, 1)
    place = jnp.arange(n_ep * places, dtype=jnp.int32)
    choose = jnp.zeros((n_ep * places, moe_rows), jnp.bool_)
    for k in range(top):
        choose = choose | (place[:, None] == destination[:, k][None, :])
    outgoing = jnp.dot(
        choose.astype(bf16), own_normed, preferred_element_type=jnp.float32
    ).astype(bf16)
    outgoing = outgoing.reshape(n_ep, places, columns)

    ff = gate_weight.shape[2]
    groups = min(RELAY_GROUPS, n_ep)
    vmem = pl.BlockSpec(memory_space=pltpu.VMEM)
    hbm = pl.BlockSpec(memory_space=pltpu.HBM)
    dma = lambda *shape: pltpu.SemaphoreType.DMA((2,) + shape)
    attention_out, back = pl.pallas_call(
        functools.partial(fused, n_ep, n_tp, heads, (PLAIN_HEAD_DIM + ROPE) ** (-0.5)),
        out_shape=(
            jax.ShapeDtypeStruct((row_count, out_proj.shape[1]), bf16),
            jax.ShapeDtypeStruct((n_ep, places, columns), bf16),
        ),
        in_specs=[vmem] * 5 + [hbm] * 3,
        out_specs=(vmem, vmem),
        scratch_shapes=[
            pltpu.VMEM((model_width, ff), bf16),
            pltpu.VMEM((model_width, ff), bf16),
            pltpu.VMEM((ff, model_width), bf16),
            pltpu.VMEM((CORES * nx, nz, share, latent + LANES), bf16),
            pltpu.VMEM((n_tp, n_ep, places, columns), bf16),
            pltpu.VMEM((n_tp, parts, row_count, LANES), bf16),
            pltpu.VMEM((n_ep * row_count, heads * LANES), bf16),
            pltpu.VMEM((n_ep // CHUNKS * places, ff), bf16),
            pltpu.VMEM((n_tp, n_ep, places, columns), bf16),
            pltpu.VMEM((n_y, n_ep, places, columns), bf16),
            pltpu.VMEM((n_y, n_ep, places, columns), bf16),
            pltpu.VMEM((n_y, n_ep, places, columns), bf16),
            pltpu.VMEM((n_ep, places, columns), bf16),
            pltpu.SemaphoreType.DMA((3,)),
            pltpu.SemaphoreType.DMA((2,)),
            dma(nz),
            dma(nz),
            dma(nx, nz),
            dma(n_ep),
            dma(n_y, groups),
            dma(n_y, groups),
            dma(n_y, parts),
            dma(n_y, parts),
            dma(n_y, CHUNKS),
            dma(n_y, CHUNKS),
            dma(n_ep),
        ],
        compiler_params=pltpu.CompilerParams(
            collective_id=0, has_side_effects=True, vmem_limit_bytes=60 * 1024 * 1024
        ),
        name="fused",
    )(
        q_all,
        lat,
        latent_to_key_value,
        wo,
        outgoing,
        gate_weight.reshape(model_width, ff),
        up_weight.reshape(model_width, ff),
        down_weight.reshape(ff, model_width),
    )
    flat_back = back.reshape(n_ep * places, columns)
    far = lax.rem(routes // nx - me // nx + nz, nz)
    step = jnp.zeros_like(far)
    for i, dz in enumerate(order):
        step = jnp.where(far == dz, i, step)
    side = lax.rem(routes % nx - me % nx + nx, nx)
    near = (step * nx + side) * places + slot.reshape(moe_rows, top)
    expert_out = jnp.zeros((moe_rows, columns), jnp.float32)
    for k in range(top):
        pick = (near[:, k][:, None] == place[None, :]).astype(bf16)
        picked = jnp.dot(pick, flat_back, preferred_element_type=jnp.float32)
        expert_out = expert_out + picked * route_weight[:, k][:, None]
    return (attention_out, expert_out.astype(bf16))


def solution(mesh):
    return jax.shard_map(
        local,
        mesh=mesh,
        in_specs=(
            P("ep", "tp"),
            P("ep", None),
            P("ep", None),
            P(),
            P(None, "tp"),
            P(None, "tp"),
            P("ep", None),
            P(),
            P("ep", None),
            P("ep", None),
            P("ep", None, "tp"),
            P("ep", None, "tp"),
            P("ep", "tp", None),
        ),
        out_specs=(P("ep", "tp"), P("ep", "tp")),
        check_vma=False,
    )
```

profile of v0, /device:TPU:15, one launch (start us, length us, event | category | flops | bytes accessed | tf_op | source)
XLA Modules:
  0.0 94.0 jit_solution(15665720205440601724)
XLA Ops:
  0.7 0.9 copy.47
  1.6 0.1 eq.92
  1.7 0.3 fusion.2
  2.1 0.1 convert_element_type.58
  2.2 0.7 broadcast_multiply_fusion
  2.9 0.1 copy.48
  3.1 0.7 broadcast_compare_fusion
  3.8 0.2 copy.54
  3.9 0.2 fusion.30
  4.2 0.3 slice_reduce_fusion
  4.5 0.8 dynamic-slice
  5.3 0.2 convert_element_type.59
  5.6 0.3 multiply_reduce_fusion
  5.9 1.4 %convolution_convert_fusion = bf16[768,512]{1,0:T(8,128)(2,1)} fusion(s32[256]{0:T(256)S(1)} %get-tuple-element.20, s32[256]{0:T(256)S(1)} %get-tuple-element.21, f32[256,2048]{1,0:T(8,128)S(1)} %convert_element_type.59, s32[]{:T(128)S(6)} %select_n.47, f32[512]{0:T(512)S(1)} %dynamic-slice, f32[256]{0:T(256)S(1)} %add_rsqrt_fusion), kind=kOutput, calls=%fused_computation.1 | convolution fusion | flops 202702848 | bytes 1315844 | tf_op jit(solution)/shard_map/dot_general | solution.py:491
  7.3 0.1 copy.57
  7.4 0.3 fusion.39
  8.1 0.8 concatenate.13.lat_ref
  8.8 0.1 multiply_cosine_fusion.1
  9.0 0.1 copy.42
  9.4 0.8 copy.56.q_ref
  10.3 79.1 %fused.1 = (bf16[256,512]{1,0:T(8,128)(2,1)}, bf16[8,96,512]{2,1,0:T(8,128)(2,1)}) custom-call(bf16[256,512]{1,0:T(8,128)(2,1)} %copy.56.q_ref, bf16[128,640]{1,0:T(8,128)(2,1)} %concatenate.13.lat_ref, bf16[512,512]{1,0:T(8,128)(2,1)} %wkv_ref.1, bf16[1024,512]{1,0:T(8,128)(2,1)} %wo_ref.1, bf16[8,96,512]{2,1,0:T(8,128)(2,1)} %bitcast.19, ...), custom_call_target="tpu_custom_call" | custom-call | tf_op jit(solution)/shard_map/fused/pallas_call | solution.py:501
  89.4 1.6 %convolution_multiply_fusion.1 = f32[256,512]{1,0:T(8,128)S(1)} fusion(bf16[768,512]{1,0:T(8,128)(2,1)} %bitcast.15, s32[256]{0:T(256)S(1)} %get-tuple-element.7, f32[256]{0:T(256)S(1)} %bitcast.21), kind=kOutput, calls=%fused_computation.4 | convolution fusion | flops 201654272 | bytes 1312768 | tf_op jit(solution)/shard_map/dot_general | solution.py:561
  91.0 2.3 %fusion.1 = bf16[256,512]{1,0:T(8,128)(2,1)} fusion(f32[256,512]{1,0:T(8,128)S(1)} %convolution_multiply_fusion.1, bf16[768,512]{1,0:T(8,128)(2,1)} %bitcast.16, s32[256]{0:T(256)S(1)} %get-tuple-element.6, f32[256]{0:T(256)S(1)} %bitcast.20), kind=kOutput, calls=%fused_computation.5 | convolution fusion | flops 201916416 | bytes 1574912 | tf_op jit(solution)/shard_map/dot_general | solution.py:561
  93.3 0.7 copy.68
  (34 shorter events, 0.6 us)
Async XLA Ops:
  0.6 6.7 %copy-start = (bf16[256,32]{0,1:T(8,128)(2,1)S(1)}, bf16[256,32]{0,1:T(8,128)(2,1)}, u32[]{:S(2)}) copy-start(bf16[256,32]{0,1:T(8,128)(2,1)} %param.15) | copy-start | bytes 49156
  0.6 4.6 %copy-start.1 = (bf16[256,2048]{1,0:T(8,128)(2,1)S(1)}, bf16[256,2048]{1,0:T(8,128)(2,1)}, u32[]{:S(2)}) copy-start(bf16[256,2048]{1,0:T(8,128)(2,1)} %param.19) | copy-start | bytes 3145732
  5.5 2.3 %copy-start.2 = (bf16[256,512]{1,0:T(8,128)(2,1)S(1)}, bf16[256,512]{1,0:T(8,128)(2,1)}, u32[]{:S(2)}) copy-start(bf16[256,512]{1,0:T(8,128)(2,1)} %param.14) | copy-start | bytes 786436
  5.5 2.4 %copy-start.5 = (f32[512]{0:T(512)S(1)}, f32[512]{0:T(512)}, u32[]{:S(2)}) copy-start(f32[512]{0:T(512)} %param.16) | copy-start | bytes 6148
  5.5 3.4 %copy-start.4 = (bf16[256,384]{1,0:T(8,128)(2,1)S(1)}, bf16[256,384]{1,0:T(8,128)(2,1)}, u32[]{:S(2)}) copy-start(bf16[256,384]{1,0:T(8,128)(2,1)} %param.13) | copy-start | bytes 589828
  10.3 79.1 %copy-start.6 = (f32[256,2]{0,1:T(2,128)S(1)}, f32[256,2]{0,1:T(2,128)}, u32[]{:S(2)}) copy-start(f32[256,2]{0,1:T(2,128)} %param.22) | copy-start | bytes 6148
  89.4 3.9 %copy-start.3 = (bf16[256,512]{1,0:T(8,128)(2,1)S(1)}, bf16[256,512]{1,0:T(8,128)(2,1)}, u32[]{:S(2)}) copy-start(bf16[256,512]{1,0:T(8,128)(2,1)} %get-tuple-element.24) | copy-start | bytes 786436
where the time goes:
time: 94.3 us; the launch traced here: 94 us
  Pallas kernels  79.1 us (84%)
  matrix products  5.54 us (6%)
  local copies, waits for them, and re-layouts  5.4 us (6%)
  other arithmetic  3 us (3%)
    pallas_call x1, Pallas kernels, local(): pl.pallas_call(functools.partial(fused, n_ep, n_tp, heads, (PLAIN_HEAD_DI...  79.1 us
    dot_general x2, matrix products, local(): picked = jnp.dot(pick, flat_back, preferred_element_type=jnp.float32)  3.84 us
    unnamed x18, local copies, waits for them, and re-layouts  1.91 us

commit v1 on v0

v1 whole, which is shorter than its diff:
```python
import functools

import jax
import jax.numpy as jnp
import numpy as np
from jax import lax
from jax.experimental import pallas as pl
from jax.experimental.pallas import tpu as pltpu
from jax.sharding import PartitionSpec as P

PLAIN_HEAD_DIM = 64
ROPE = 32
VALUE_HEAD_DIM = 64
LANES = 128
CORES = 2


EPSILON = 1e-06
ROPE_BASE_VALUE = 10000.0


def ep_shape(n_ep):
    nx = 2 if n_ep % 2 == 0 else 1
    return nx, n_ep // nx


def partners(nz):
    side = lambda z: 2 * z < nz
    return [
        sorted(
            (o for o in range(nz) if o != z),
            key=lambda o: (abs(o - z), side(o) != side(z), o),
        )
        for z in range(nz)
    ]


def merge_rows(block):
    return block.reshape(block.shape[0] * block.shape[1], block.shape[2])


def fused(
    n_ep,
    n_tp,
    heads,
    scale,
    routes_ref,
    weight_ref,
    mgain_ref,
    lgain_ref,
    rope_ref,
    moe_hbm,
    ckv_hbm,
    q_hbm,
    wkv_hbm,
    wo_hbm,
    wg_hbm,
    wu_hbm,
    wd_hbm,
    att_out,
    exp_out,
    moe_v,
    ckv_v,
    qraw,
    wkv_ref,
    wo_ref,
    wg,
    wu,
    wd,
    normed,
    key_ref,
    mix_ref,
    out_z,
    out_x,
    rope_v,
    q_ref,
    g_lat,
    g_moe,
    g_att,
    kv,
    hidden,
    part,
    r1,
    s2,
    r2,
    tot,
    back,
    in_sem,
    lat_up,
    lat_dn,
    lat_x,
    lat_c,
    moe_a,
    moe_x,
    moe_xc,
    moe_y,
    moe_c,
    att_y,
    att_c,
    red_c,
    red_y,
    ret_a,
):
    f32, bf16 = jnp.float32, jnp.bfloat16
    frequency_of = ROPE_BASE_VALUE ** (-np.arange(ROPE // 2, dtype=np.float32) * 2.0 / ROPE)
    me = lax.axis_index("ep")
    tp = lax.axis_index("tp")
    n_y = n_tp // CORES
    my_y = tp // CORES
    my_c = lax.rem(tp, CORES)
    mate = my_y * CORES + (1 - my_c)
    nx, nz = ep_shape(n_ep)
    my_z = me // nx
    my_x = lax.rem(me, nx)
    row_count, model_width = moe_v.shape
    columns = model_width // n_tp
    cap = g_moe.shape[2]
    chunks = nz
    rows = nx * cap
    ff = wg.shape[1]
    tile = min(256, ff)
    tiles = ff // tile
    share = ckv_v.shape[0]
    latent = ckv_v.shape[1]
    sends = []

    zs = [my_z]
    for i in range(nz - 1):
        value = jnp.int32(0)
        for z, others in enumerate(partners(nz)):
            value = jnp.where(my_z == z, others[i], value)
        zs.append(value)

    def slot(i, dx):
        return zs[i] * nx + dx

    def at(i, dx):
        return zs[i] * nx + lax.rem(my_x + dx, nx)

    def seen(dx):
        return my_z * nx + (nx - dx) % nx

    def remote(src, dst, sems, sent, got, ep_id, tp_id):
        return pltpu.make_async_remote_copy(
            src_ref=src,
            dst_ref=dst,
            send_sem=sems.at[(0,) + sent],
            recv_sem=sems.at[(1,) + got],
            device_id=(ep_id, tp_id),
            device_id_type=pl.DeviceIdType.MESH,
        )

    def to(src, dst, sems, index, ep_id, tp_id, got=None):
        copy = remote(src, dst, sems, index, index if got is None else got, ep_id, tp_id)
        copy.start()
        sends.append(copy)
        return copy

    def come(dst, sems, got):
        remote(dst, dst, sems, got, got, me, mate).wait_recv()

    def lane_block(t):
        return pl.ds(pl.multiple_of(t * columns, columns), columns)

    S = jax.named_scope

    barrier = pltpu.get_barrier_semaphore()
    for d in range(1, n_ep):
        pl.semaphore_signal(
            barrier,
            inc=1,
            device_id=(lax.rem(me + d, n_ep), tp),
            device_id_type=pl.DeviceIdType.MESH,
        )
    for d in range(1, n_tp):
        pl.semaphore_signal(
            barrier,
            inc=1,
            device_id=(me, lax.rem(tp + d, n_tp)),
            device_id_type=pl.DeviceIdType.MESH,
        )

    loads = []
    half_rows = pl.ds(pl.multiple_of(my_c * share, share), share)
    for i, (source, target) in enumerate(
        (
            (moe_hbm, moe_v),
            (ckv_hbm.at[half_rows], ckv_v),
            (q_hbm, qraw),
            (wg_hbm, wg),
            (wu_hbm, wu),
            (wd_hbm, wd),
            (wkv_hbm, wkv_ref),
            (wo_hbm, wo_ref),
        )
    ):
        copy = pltpu.make_async_copy(source, target, in_sem.at[i])
        loads.append(copy)
    loads[0].start()

    with S("routing"):
        top = routes_ref.shape[0]
        expert_of = lax.broadcasted_iota(jnp.int32, (n_ep, row_count), 0)
        named = jnp.zeros((n_ep, row_count), f32)
        mix = jnp.zeros((n_ep, row_count), f32)
        for k in range(top):
            hit = routes_ref[k : k + 1, :] == expert_of
            named = jnp.where(hit, 1.0, named)
            mix = jnp.where(hit, weight_ref[k : k + 1, :], mix)
        mix_ref[...] = mix
        first = lax.broadcasted_iota(jnp.int32, (row_count, row_count), 0)
        second = lax.broadcasted_iota(jnp.int32, (row_count, row_count), 1)
        before = jnp.where(first < second, 1.0, 0.0).astype(bf16)
        earlier = jnp.dot(named.astype(bf16), before, preferred_element_type=f32)
        key_ref[...] = jnp.where(named > 0.5, earlier, -1.0).astype(jnp.int32)
    place = lax.broadcasted_iota(jnp.int32, (cap, row_count), 0)

    def chosen(e):
        return key_ref[pl.ds(e, 1), :] == place

    def rows_for(e, cols):
        pick = jnp.where(chosen(e), 1.0, 0.0).astype(bf16)
        return jnp.dot(pick, normed[:, cols], preferred_element_type=f32).astype(bf16)

    with S("norm"):
        loads[0].wait()
        for copy in loads[1:]:
            copy.start()
        step_rows = 16

        def norm(i, carry):
            span = pl.ds(pl.multiple_of(i * step_rows, step_rows), step_rows)
            x = moe_v[span, :].astype(f32)
            level = lax.rsqrt(jnp.mean(x * x, axis=-1, keepdims=True) + EPSILON)
            normed[span, :] = (x * level * mgain_ref[...]).astype(bf16)
            return carry

        lax.fori_loop(0, row_count // step_rows, norm, 0, unroll=4)

    with S("gather_x"):
        for dx in range(1, nx):
            for o in range(n_y):
                out_x[dx, o] = rows_for(at(0, dx), lane_block(o * CORES + my_c))
    with S("barrier"):
        pl.semaphore_wait(barrier, n_ep + n_tp - 2)
    for dx in range(1, nx):
        for o in range(n_y):
            t = o * CORES + my_c
            to(
                out_x.at[dx, o],
                g_moe.at[t, seen(dx)],
                moe_x,
                (dx, o),
                at(0, dx),
                tp,
                ((nx - dx) % nx, o),
            )
    with S("gather_z"):
        for i in range(1, nz):
            for dx in range(nx):
                n = i * nx + dx
                out_z[n] = rows_for(at(i, dx), lane_block(tp))
                to(out_z.at[n], g_moe.at[tp, seen(dx)], moe_a, (n,), at(i, dx), tp, (seen(dx),))
    with S("gather_own"):
        for t in range(n_tp):
            g_moe[t, slot(0, 0)] = rows_for(me, slice(t * columns, (t + 1) * columns))

    with S("prep"):
        half = ROPE // 2
        pos = (me * row_count + lax.broadcasted_iota(jnp.int32, (half, row_count), 1)).astype(f32)
        band = lax.broadcasted_iota(jnp.int32, (half, row_count), 0)
        frequency = jnp.zeros((half, row_count), f32)
        for i in range(half):
            frequency = jnp.where(band == i, float(np.float32(frequency_of[i])), frequency)
        angle = pos * frequency
        cosine, sine = jnp.cos(angle), jnp.sin(angle)
        zero = lambda n: jnp.zeros((n, row_count), f32)
        rest = LANES - PLAIN_HEAD_DIM - ROPE
        cos_t = jnp.concatenate(
            [jnp.ones((PLAIN_HEAD_DIM, row_count), f32), cosine, cosine, zero(rest)], axis=0
        ).T
        down_t = jnp.concatenate([zero(PLAIN_HEAD_DIM), -sine, zero(half + rest)], axis=0).T
        up_t = jnp.concatenate([zero(PLAIN_HEAD_DIM + half), sine, zero(rest)], axis=0).T
        shared = rope_ref[...].astype(f32)
        first_half, second_half = shared[:half], shared[half:]
        rope_v[...] = jnp.concatenate(
            [
                zero(PLAIN_HEAD_DIM),
                first_half * cosine - second_half * sine,
                second_half * cosine + first_half * sine,
                zero(rest),
            ],
            axis=0,
        )
        own_lat = my_c * nx
        loads[1].wait()
        c = ckv_v[...].astype(f32)
        level = lax.rsqrt(jnp.mean(c * c, axis=-1, keepdims=True) + EPSILON)
        own_block = g_lat.at[own_lat, my_z]
        own_block[:, :latent] = (c * level * lgain_ref[...]).astype(bf16)
        own_block[:, latent:] = rope_v[:, half_rows].T.astype(bf16)
        loads[2].wait()
        width = PLAIN_HEAD_DIM + ROPE
        for h in range(heads):
            start = (h * width) // LANES * LANES
            shift = h * width - start
            size = LANES if shift + width <= LANES else 2 * LANES
            x = qraw[:, start : start + size].astype(f32)
            if shift:
                x = pltpu.roll(x, size - shift, 1)
            x = x[:, :LANES]
            q_ref[:, h * LANES : (h + 1) * LANES] = (
                x * cos_t + pltpu.roll(x, LANES - half, 1) * down_t + pltpu.roll(x, half, 1) * up_t
            ).astype(bf16)

    lat_over, lat_side = {}, {}

    def lat_hop(d):
        if d == 0:
            src = g_lat.at[own_lat, my_z]

            @pl.when(my_z + 1 < nz)
            def _():
                remote(src, src, lat_up, (my_z,), (my_z,), me + nx, tp).start()

            @pl.when(my_z > 0)
            def _():
                remote(src, src, lat_dn, (my_z,), (my_z,), me - nx, tp).start()

            lat_share(my_z)
        else:
            @pl.when(my_z >= d)
            def _():
                z = my_z - d
                src = g_lat.at[own_lat, z]
                come(src, lat_up, (z,))

                @pl.when(my_z + 1 < nz)
                def _():
                    remote(src, src, lat_up, (z,), (z,), me + nx, tp).start()

                lat_share(z)

            @pl.when(my_z + d < nz)
            def _():
                z = my_z + d
                src = g_lat.at[own_lat, z]
                come(src, lat_dn, (z,))

                @pl.when(my_z > 0)
                def _():
                    remote(src, src, lat_dn, (z,), (z,), me - nx, tp).start()

                lat_share(z)

    def lat_share(z):
        mine = g_lat.at[own_lat, z]
        remote(mine, mine, lat_c, (0, z), (0, z), me, mate).start()
        if nx > 1:
            side = g_lat.at[own_lat + 1, z]
            remote(mine, side, lat_x, (z,), (z,), my_z * nx + 1 - my_x, tp).start()

    def lat_cross(z):
        if nx > 1:
            side = g_lat.at[own_lat + 1, z]
            come(side, lat_x, (z,))
            remote(side, side, lat_c, (1, z), (1, z), me, mate).start()

    def lat_done(z):
        for i in range(nx):
            come(g_lat.at[(1 - my_c) * nx + i, z], lat_c, (i, z))

    def lat_drain():
        for z in range(nz):
            block = g_lat.at[own_lat, z]

            @pl.when(jnp.logical_and(my_z >= z, my_z + 1 < nz))
            def _():
                remote(block, block, lat_up, (z,), (z,), me, mate).wait_send()

            @pl.when(jnp.logical_and(my_z <= z, my_z > 0))
            def _():
                remote(block, block, lat_dn, (z,), (z,), me, mate).wait_send()

            remote(block, block, lat_c, (0, z), (0, z), me, mate).wait_send()
            if nx > 1:
                side = g_lat.at[own_lat + 1, z]
                remote(block, block, lat_x, (z,), (z,), me, mate).wait_send()
                remote(side, side, lat_c, (1, z), (1, z), me, mate).wait_send()

    relay_y, relay_c = {}, {}

    def x_arrive():
        for dx in range(1, nx):
            relay_c[0, dx] = []
            for o in range(n_y):
                block = g_moe.at[o * CORES + my_c, slot(0, dx)]
                come(block, moe_x, (dx, o))
                relay_c[0, dx].append(to(block, block, moe_xc, (dx, o), me, mate))

    def spread(i, dx):
        n = i * nx + dx
        block = g_moe.at[tp, slot(i, dx)]
        come(block, moe_a, (slot(i, dx),))
        for o in range(1, n_y):
            other = lax.rem(my_y + o, n_y) * CORES + my_c
            relay_y[n, o] = to(block, block, moe_y, (o, n), me, other)
        relay_c[i, dx] = [to(block, block, moe_c, (0, n), me, mate)]

    def forward(i, dx):
        n = i * nx + dx
        for o in range(1, n_y):
            relay_y[n, o].wait_recv()
            came = g_moe.at[lax.rem(my_y + n_y - o, n_y) * CORES + my_c, slot(i, dx)]
            relay_c[i, dx].append(to(came, came, moe_c, (o, n), me, mate))

    def finish(i):
        for dx in range(nx):
            for copy in relay_c.get((i, dx), ()):
                copy.wait_recv()

    def up(c, f):
        span = slice(f * tile, (f + 1) * tile)
        gate = jnp.zeros((rows, tile), f32)
        lift = jnp.zeros((rows, tile), f32)
        for t in range(n_tp):
            x = merge_rows(g_moe[t, pl.ds(zs[c] * nx, nx)])
            gate += jnp.dot(
                x, wg[t * columns : (t + 1) * columns, span], preferred_element_type=f32
            )
            lift += jnp.dot(
                x, wu[t * columns : (t + 1) * columns, span], preferred_element_type=f32
            )
        hidden[:, span] = (gate / (1.0 + jnp.exp(-gate)) * lift).astype(bf16)

    reduce_c, reduce_y = {}, {}

    def down(c):
        for o in list(range(1, n_y)) + [0]:
            y = lax.rem(my_y + o, n_y)
            for mine in range(2):
                t = y * CORES + (my_c if mine else 1 - my_c)
                part[t, c] = (
                    jnp.dot(hidden[...], wd[:, lane_block(t)], preferred_element_type=f32)
                    .astype(bf16)
                    .reshape(nx, cap, columns)
                )
                if not mine:
                    reduce_c[c, o] = to(part.at[t, c], r1.at[o, c], red_c, (o, c), me, mate)

    def level_two(c):
        for o in range(1, n_y):
            y = lax.rem(my_y + o, n_y)
            reduce_c[c, o].wait_recv()
            for dx in range(nx):
                n = c * nx + dx
                s2[o, c, dx] = (
                    part[y * CORES + my_c, c, dx].astype(f32) + r1[o, c, dx].astype(f32)
                ).astype(bf16)
                reduce_y[n, o] = to(
                    s2.at[o, c, dx], r2.at[o, c, dx], red_y, (o, n), me, y * CORES + my_c
                )

    def give_back(c):
        reduce_c[c, 0].wait_recv()
        for dx in range(nx):
            n = c * nx + dx
            total = part[tp, c, dx].astype(f32) + r1[0, c, dx].astype(f32)
            for o in range(1, n_y):
                reduce_y[n, o].wait_recv()
                total += r2[o, c, dx].astype(f32)
            tot[n] = total.astype(bf16)
            if n > 0:
                to(tot.at[n], back.at[seen(dx)], ret_a, (n,), at(c, dx), tp, (seen(dx),))

    def combine(i, dx):
        if i == 0 and dx == 0:
            came = tot[0]
        else:
            come(back.at[slot(i, dx)], ret_a, (slot(i, dx),))
            came = back[slot(i, dx)]
        e = at(i, dx)
        weight = jnp.where(chosen(e), mix_ref[pl.ds(e, 1), :], 0.0)
        high = weight.astype(bf16)
        low = (weight - high.astype(f32)).astype(bf16)
        add = lax.dot_general(
            jnp.concatenate([high, low], axis=0),
            jnp.concatenate([came, came], axis=0),
            (((0,), (0,)), ((), ())),
            preferred_element_type=f32,
        )
        if i == 0 and dx == 0:
            exp_out[...] = add
        else:
            exp_out[...] += add

    block = nz * share

    def expand(t, carry):
        kv[pl.ds(pl.multiple_of(t * block, block), block), :] = jnp.dot(
            merge_rows(g_lat[t])[:, :latent], wkv_ref[...], preferred_element_type=f32
        ).astype(bf16)
        return carry

    whole_lat = g_lat.reshape(g_lat.shape[0] * block, g_lat.shape[3])
    lane = lax.broadcasted_iota(jnp.int32, (1, LANES), 1)
    packed = 2 if heads % 2 == 0 else 1
    parts = heads // packed
    att_in, att_mate = [], []

    def attend(part_index):
        for h in range(part_index * packed, (part_index + 1) * packed):
            head = kv[:, h * LANES : (h + 1) * LANES]
            keys = jnp.where(lane < PLAIN_HEAD_DIM, head, whole_lat[:, latent : latent + LANES])
            scores = (
                lax.dot_general(
                    q_ref[:, h * LANES : (h + 1) * LANES],
                    keys,
                    (((1,), (1,)), ((), ())),
                    preferred_element_type=f32,
                )
                * scale
            )
            peak = jnp.max(scores, axis=-1, keepdims=True)
            e = jnp.exp(scores - peak)
            total = jnp.sum(e, axis=-1, keepdims=True)
            mixed = jnp.dot(e.astype(bf16), head, preferred_element_type=f32) / total
            if packed == 1:
                mixed = jnp.where(lane < PLAIN_HEAD_DIM, 0.0, mixed)
            elif h % 2 == 0:
                held = pltpu.roll(mixed, VALUE_HEAD_DIM, 1)
            else:
                mixed = jnp.where(lane < VALUE_HEAD_DIM, held, mixed)
        g_att[tp, part_index] = mixed.astype(bf16)

    def att_send(p):
        own = g_att.at[tp, p]
        for o in range(1, n_y):
            other = lax.rem(my_y + o, n_y) * CORES + my_c
            att_in.append((p, o, to(own, own, att_y, (o, p), me, other)))
        att_mate.append(to(own, own, att_c, (0, p), me, mate))

    def att_forward(part_index):
        for p, o, copy in att_in:
            if p == part_index:
                copy.wait_recv()
                came = g_att.at[lax.rem(my_y + n_y - o, n_y) * CORES + my_c, p]
                att_mate.append(to(came, came, att_c, (o, p), me, mate))

    def project():
        for copy in att_mate:
            copy.wait_recv()
        total = jnp.zeros(att_out.shape, f32)
        for t in range(n_tp):
            x = jnp.concatenate([g_att[t, p] for p in range(g_att.shape[1])], axis=1)
            width = x.shape[1]
            total += jnp.dot(x, wo_ref[t * width : (t + 1) * width, :], preferred_element_type=f32)
        att_out[...] = total

    def weights_in():
        for copy in loads[3:]:
            copy.wait()

    def scoped(name, f, *a):
        with S(name):
            f(*a)

    def each(name, f, i):
        for dx in range(nx):
            scoped("%s%d%d" % (name, i, dx), f, i, dx)

    def half_up(c, k):
        for f in range(tiles):
            if (2 * f) // tiles == k:
                scoped("up%d_%d" % (c, f), up, c, f)

    last = nz - 1
    scoped("x_arrive", x_arrive)
    if nz > 1:
        each("spread", spread, 1)
    scoped("weights", weights_in)
    lat_next = 0
    for c in range(nz):
        scoped("finish%d" % c, finish, c)
        half_up(c, 0)
        if c == 0 and nz > 1:
            scoped("forward10", forward, 1, 0)
        if 1 <= c and 2 < c + 1 < nz + 0:
            scoped("spread%d0" % (c + 1), spread, c + 1, 0)
        half_up(c, 1)
        if 1 <= c and 2 < c + 1 < nz + 0:
            for dx in range(1, nx):
                scoped("spread%d%d" % (c + 1, dx), spread, c + 1, dx)
        if c > 0:
            scoped("level_two%d" % (c - 1), level_two, c - 1)
        scoped("down%d" % c, down, c)
        if c == 0 and nz > 1:
            for dx in range(1, nx):
                scoped("forward1%d" % dx, forward, 1, dx)
        if 1 <= c and 2 < c + 1 < nz + 0:
            each("forward", forward, c + 1)
        if c == 0 and nz > 2:
            each("spread", spread, 2)
            each("forward", forward, 2)
        if c > 0:
            scoped("give_back%d" % (c - 1), give_back, c - 1)
            scoped("lat%d" % lat_next, lat_hop, lat_next)
            lat_next += 1
    scoped("level_two%d" % last, level_two, last)
    while lat_next < nz:
        scoped("lat%d" % lat_next, lat_hop, lat_next)
        lat_next += 1
    scoped("give_back%d" % last, give_back, last)
    each("combine", combine, 0)
    for z in range(nz):
        scoped("cross%d" % z, lat_cross, z)
    for z in range(nz):
        scoped("lat_done%d" % z, lat_done, z)
    with S("expand"):
        lax.fori_loop(0, g_lat.shape[0], expand, 0)
    for p in range(parts):
        scoped("attend%d" % p, attend, p)
        att_send(p)
    for i in range(1, nz - 1):
        each("combine", combine, i)
    for p in range(parts):
        scoped("att_forward%d" % p, att_forward, p)
    scoped("project", project)
    if nz > 1:
        each("combine", combine, last)
    for copy in sends:
        copy.wait_send()
    lat_drain()


def local(
    queries,
    compressed_key_value,
    rope_key,
    latent_norm_gain,
    latent_to_key_value,
    out_proj,
    moe_input,
    moe_gain,
    routes,
    route_weight,
    gate_weight,
    up_weight,
    down_weight,
):
    n_ep = lax.axis_size("ep")
    n_tp = lax.axis_size("tp")
    n_y = n_tp // CORES
    bf16 = jnp.bfloat16
    row_count = queries.shape[0]
    heads = latent_to_key_value.shape[1] // (PLAIN_HEAD_DIM + VALUE_HEAD_DIM)
    latent = compressed_key_value.shape[1]
    share = row_count // CORES
    nx, nz = ep_shape(n_ep)
    over = -queries.shape[1] % LANES
    if over:
        queries = jnp.pad(queries, ((0, 0), (0, over)))
    if heads % 2 == 0:
        wo = out_proj
        parts = heads // 2
    else:
        wo = out_proj.reshape(n_tp * heads, VALUE_HEAD_DIM, out_proj.shape[1])
        wo = jnp.concatenate([jnp.zeros_like(wo), wo], axis=1)
        wo = wo.reshape(n_tp * heads * LANES, out_proj.shape[1])
        parts = heads
    model_width = moe_input.shape[1]
    capacity = 3 * row_count // n_ep
    places = -(-capacity // 16) * 16
    columns = model_width // n_tp
    ff = gate_weight.shape[2]
    vmem = pl.BlockSpec(memory_space=pltpu.VMEM)
    hbm = pl.BlockSpec(memory_space=pltpu.HBM)
    dma = lambda *shape: pltpu.SemaphoreType.DMA((2,) + shape)
    attention, experts = pl.pallas_call(
        functools.partial(fused, n_ep, n_tp, heads, (PLAIN_HEAD_DIM + ROPE) ** (-0.5)),
        out_shape=(
            jax.ShapeDtypeStruct((row_count, out_proj.shape[1]), jnp.float32),
            jax.ShapeDtypeStruct((row_count, columns), jnp.float32),
        ),
        in_specs=[vmem] * 5 + [hbm] * 8,
        out_specs=(vmem, vmem),
        scratch_shapes=[
            pltpu.VMEM((row_count, model_width), bf16),
            pltpu.VMEM((share, latent), bf16),
            pltpu.VMEM(queries.shape, bf16),
            pltpu.VMEM(latent_to_key_value.shape, bf16),
            pltpu.VMEM(wo.shape, bf16),
            pltpu.VMEM((model_width, ff), bf16),
            pltpu.VMEM((model_width, ff), bf16),
            pltpu.VMEM((ff, model_width), bf16),
            pltpu.VMEM((row_count, model_width), bf16),
            pltpu.VMEM((n_ep, row_count), jnp.int32),
            pltpu.VMEM((n_ep, row_count), jnp.float32),
            pltpu.VMEM((n_ep, places, columns), bf16),
            pltpu.VMEM((nx, n_y, places, columns), bf16),
            pltpu.VMEM((LANES, row_count), jnp.float32),
            pltpu.VMEM((row_count, heads * LANES), bf16),
            pltpu.VMEM((CORES * nx, nz, share, latent + LANES), bf16),
            pltpu.VMEM((n_tp, n_ep, places, columns), bf16),
            pltpu.VMEM((n_tp, parts, row_count, LANES), bf16),
            pltpu.VMEM((n_ep * row_count, heads * LANES), bf16),
            pltpu.VMEM((nx * places, ff), bf16),
            pltpu.VMEM((n_tp, nz, nx, places, columns), bf16),
            pltpu.VMEM((n_y, nz, nx, places, columns), bf16),
            pltpu.VMEM((n_y, nz, nx, places, columns), bf16),
            pltpu.VMEM((n_y, nz, nx, places, columns), bf16),
            pltpu.VMEM((n_ep, places, columns), bf16),
            pltpu.VMEM((n_ep, places, columns), bf16),
            pltpu.SemaphoreType.DMA((8,)),
            dma(nz),
            dma(nz),
            dma(nz),
            dma(nx, nz),
            dma(n_ep),
            dma(nx, n_y),
            dma(nx, n_y),
            dma(n_y, n_ep),
            dma(n_y, n_ep),
            dma(n_y, parts),
            dma(n_y, parts),
            dma(n_y, nz),
            dma(n_y, n_ep),
            dma(n_ep),
        ],
        compiler_params=pltpu.CompilerParams(
            collective_id=0, has_side_effects=True, vmem_limit_bytes=50 * 1024 * 1024
        ),
        name="fused",
    )(
        routes.T,
        route_weight.T,
        moe_gain.reshape(1, model_width),
        latent_norm_gain.reshape(1, latent),
        rope_key.T,
        moe_input,
        compressed_key_value,
        queries,
        latent_to_key_value,
        wo,
        gate_weight.reshape(model_width, ff),
        up_weight.reshape(model_width, ff),
        down_weight.reshape(ff, model_width),
    )
    return attention.astype(bf16), experts.astype(bf16)


def solution(mesh):
    return jax.shard_map(
        local,
        mesh=mesh,
        in_specs=(
            P("ep", "tp"),
            P("ep", None),
            P("ep", None),
            P(),
            P(None, "tp"),
            P(None, "tp"),
            P("ep", None),
            P(),
            P("ep", None),
            P("ep", None),
            P("ep", None, "tp"),
            P("ep", None, "tp"),
            P("ep", "tp", None),
        ),
        out_specs=(P("ep", "tp"), P("ep", "tp")),
        check_vma=False,
    )
```

time: 94.3 us -> 84.8 us (0.90)
  the two profiles are of different devices: /device:TPU:15 before, /device:TPU:0 now
where the time goes in v1:
time: 84.8 us; the launch traced here: 84.4 us
  Pallas kernels  74.7 us (88%)
  local copies, waits for them, and re-layouts  7.59 us (9%)
  other arithmetic  1.47 us (2%)
    pallas_call x1, Pallas kernels, local(): pl.pallas_call(functools.partial(fused, n_ep, n_tp, heads, (PLAIN_HEAD_DI...  74.7 us
    unnamed x18, local copies, waits for them, and re-layouts  7.59 us

profile of v1, /device:TPU:0, one launch (start us, length us, event | category | flops | bytes accessed | tf_op | source)
XLA Modules:
  0.0 84.4 jit_solution(4701290389135258823)
XLA Ops:
  0.6 0.0 copy-start
  0.6 1.2 %copy-done = bf16[256,2048]{1,0:T(8,128)(2,1)S(1)} copy-done((bf16[256,2048]{1,0:T(8,128)(2,1)S(1)}, bf16[256,2048]{1,0:T(8,128)(2,1)}, u32[]{:S(2)}) %copy-start) | copy-done | bytes 1048600
  1.9 0.0 copy-start.1
  1.9 1.0 %copy-done.1 = bf16[512,512]{1,0:T(8,128)(2,1)S(1)} copy-done((bf16[512,512]{1,0:T(8,128)(2,1)S(1)}, bf16[512,512]{1,0:T(8,128)(2,1)}, u32[]{:S(2)}) %copy-start.1) | copy-done | bytes 524312
  2.9 0.0 copy-start.2
  2.9 0.9 %copy-done.2 = bf16[256,512]{1,0:T(8,128)(2,1)S(1)} copy-done((bf16[256,512]{1,0:T(8,128)(2,1)S(1)}, bf16[256,512]{1,0:T(8,128)(2,1)}, u32[]{:S(2)}) %copy-start.2) | copy-done | bytes 262168
  3.9 0.0 copy-start.3
  3.9 0.9 %copy-done.3 = bf16[256,384]{1,0:T(8,128)(2,1)S(1)} copy-done((bf16[256,384]{1,0:T(8,128)(2,1)S(1)}, bf16[256,384]{1,0:T(8,128)(2,1)}, u32[]{:S(2)}) %copy-start.3) | copy-done | bytes 196632
  4.8 0.0 copy-start.4
  4.8 0.7 copy-done.4
  5.5 0.0 copy-start.5
  5.5 0.7 copy-done.5
  6.2 0.0 copy-start.6
  6.2 0.7 copy-done.6
  6.9 0.0 copy-start.7
  6.9 0.7 copy-done.7
  7.6 0.0 copy-start.8
  7.6 0.7 copy-done.8
  8.2 74.7 %fused.1 = (f32[256,512]{1,0:T(8,128)S(1)}, f32[256,512]{1,0:T(8,128)S(1)}) custom-call(s32[2,256]{1,0:T(2,128)S(1)} %bitcast.10, f32[2,256]{1,0:T(2,128)S(1)} %bitcast.11, f32[1,2048]{1,0:T(1,128)S(1)} %bitcast.9, f32[1,512]{1,0:T(1,128)S(1)} %bitcast.12, bf16[32,256]{1,0:T(8,128)(2,1)S(1)} %bitcast.8, bf16[256,2048]{1,0:T(8,128)(2,1)S(1)} %copy-done, ...), custom_call_target="tpu_custom_call" | custom-call | tf_op jit(solution)/shard_map/fused/pallas_call | solution.py:679
  82.9 0.7 convert_element_type.6
  83.7 0.7 convert_element_type.7
Async XLA Ops:
  0.6 1.2 %copy-start = (bf16[256,2048]{1,0:T(8,128)(2,1)S(1)}, bf16[256,2048]{1,0:T(8,128)(2,1)}, u32[]{:S(2)}) copy-start(bf16[256,2048]{1,0:T(8,128)(2,1)} %moe_hbm.1) | copy-start | bytes 3145732
  1.9 1.0 %copy-start.1 = (bf16[512,512]{1,0:T(8,128)(2,1)S(1)}, bf16[512,512]{1,0:T(8,128)(2,1)}, u32[]{:S(2)}) copy-start(bf16[512,512]{1,0:T(8,128)(2,1)} %wkv_hbm.1) | copy-start | bytes 1572868
  2.9 0.9 %copy-start.2 = (bf16[256,512]{1,0:T(8,128)(2,1)S(1)}, bf16[256,512]{1,0:T(8,128)(2,1)}, u32[]{:S(2)}) copy-start(bf16[256,512]{1,0:T(8,128)(2,1)} %ckv_hbm.1) | copy-start | bytes 786436
  3.9 0.9 %copy-start.3 = (bf16[256,384]{1,0:T(8,128)(2,1)S(1)}, bf16[256,384]{1,0:T(8,128)(2,1)}, u32[]{:S(2)}) copy-start(bf16[256,384]{1,0:T(8,128)(2,1)} %q_hbm.1) | copy-start | bytes 589828
  4.8 0.7 copy-start.4
  5.5 0.7 copy-start.5
  6.2 0.7 copy-start.6
  6.9 0.7 copy-start.7
  7.6 0.7 copy-start.8

commit v2 on v1

--- a/solution.py
+++ b/solution.py
@@ -44,11 +44,11 @@
     n_tp,
     heads,
     scale,
-    routes_ref,
-    weight_ref,
-    mgain_ref,
-    lgain_ref,
-    rope_ref,
+    routes_hbm,
+    weight_hbm,
+    mgain_hbm,
+    lgain_hbm,
+    rope_hbm,
     moe_hbm,
     ckv_hbm,
     q_hbm,
@@ -59,6 +59,11 @@
     wd_hbm,
     att_out,
     exp_out,
+    routes_ref,
+    weight_ref,
+    mgain_ref,
+    lgain_ref,
+    rope_ref,
     moe_v,
     ckv_v,
     qraw,
@@ -164,6 +169,10 @@
 
     S = jax.named_scope
 
+    def scoped(name, f, *a):
+        with S(name):
+            f(*a)
+
     barrier = pltpu.get_barrier_semaphore()
     for d in range(1, n_ep):
         pl.semaphore_signal(
@@ -181,6 +190,19 @@
         )
 
     loads = []
+    small = []
+    for i, (source, target) in enumerate(
+        (
+            (routes_hbm, routes_ref),
+            (weight_hbm, weight_ref),
+            (mgain_hbm, mgain_ref),
+            (lgain_hbm, lgain_ref),
+            (rope_hbm, rope_ref),
+        )
+    ):
+        copy = pltpu.make_async_copy(source, target, in_sem.at[8 + i])
+        copy.start()
+        small.append(copy)
     half_rows = pl.ds(pl.multiple_of(my_c * share, share), share)
     for i, (source, target) in enumerate(
         (
@@ -199,6 +221,8 @@
     loads[0].start()
 
     with S("routing"):
+        for copy in small[:2]:
+            copy.wait()
         top = routes_ref.shape[0]
         expert_of = lax.broadcasted_iota(jnp.int32, (n_ep, row_count), 0)
         named = jnp.zeros((n_ep, row_count), f32)
@@ -224,6 +248,8 @@
 
     with S("norm"):
         loads[0].wait()
+        for copy in small[2:]:
+            copy.wait()
         for copy in loads[1:]:
             copy.start()
         step_rows = 16
@@ -237,30 +263,64 @@
 
         lax.fori_loop(0, row_count // step_rows, norm, 0, unroll=4)
 
-    with S("gather_x"):
-        for dx in range(1, nx):
+
+    def direct(i, dx):
+        return i == 0 or (i == 1 and dx == 0)
+
+    sent = {}
+
+    def gather(i, dx):
+        n = i * nx + dx
+        if direct(i, dx):
             for o in range(n_y):
-                out_x[dx, o] = rows_for(at(0, dx), lane_block(o * CORES + my_c))
+                out_x[n, o] = rows_for(at(i, dx), lane_block(o * CORES + my_c))
+        else:
+            out_z[n] = rows_for(at(i, dx), lane_block(tp))
+
+    def send(i, dx):
+        n = i * nx + dx
+        if direct(i, dx):
+            sent[n] = [
+                to(
+                    out_x.at[n, o],
+                    g_moe.at[o * CORES + my_c, seen(dx)],
+                    moe_x,
+                    (n, o),
+                    at(i, dx),
+                    tp,
+                    (seen(dx), o),
+                )
+                for o in range(n_y)
+            ]
+        else:
+            sent[n] = [
+                to(out_z.at[n], g_moe.at[tp, seen(dx)], moe_a, (n,), at(i, dx), tp, (seen(dx),))
+            ]
+
+    def gone(i, dx):
+        for copy in sent[i * nx + dx]:
+            copy.wait_send()
+            sends[:] = [other for other in sends if other is not copy]
+
+    side = range(1, nx)
+    with S("gather_a"):
+        for dx in side:
+            gather(0, dx)
+        if nz > 1:
+            gather(1, 0)
+        if nz > 2:
+            gather(2, 0)
     with S("barrier"):
         pl.semaphore_wait(barrier, n_ep + n_tp - 2)
-    for dx in range(1, nx):
-        for o in range(n_y):
-            t = o * CORES + my_c
-            to(
-                out_x.at[dx, o],
-                g_moe.at[t, seen(dx)],
-                moe_x,
-                (dx, o),
-                at(0, dx),
-                tp,
-                ((nx - dx) % nx, o),
-            )
-    with S("gather_z"):
+    for dx in side:
+        send(0, dx)
+    for i in range(1, min(3, nz)):
+        send(i, 0)
+    with S("gather_b"):
         for i in range(1, nz):
             for dx in range(nx):
-                n = i * nx + dx
-                out_z[n] = rows_for(at(i, dx), lane_block(tp))
-                to(out_z.at[n], g_moe.at[tp, seen(dx)], moe_a, (n,), at(i, dx), tp, (seen(dx),))
+                if dx or i > 2:
+                    gather(i, dx)
     with S("gather_own"):
         for t in range(n_tp):
             g_moe[t, slot(0, 0)] = rows_for(me, slice(t * columns, (t + 1) * columns))
@@ -390,13 +450,12 @@
 
     relay_y, relay_c = {}, {}
 
-    def x_arrive():
-        for dx in range(1, nx):
-            relay_c[0, dx] = []
-            for o in range(n_y):
-                block = g_moe.at[o * CORES + my_c, slot(0, dx)]
-                come(block, moe_x, (dx, o))
-                relay_c[0, dx].append(to(block, block, moe_xc, (dx, o), me, mate))
+    def arrive(i, dx):
+        relay_c[i, dx] = []
+        for o in range(n_y):
+            block = g_moe.at[o * CORES + my_c, slot(i, dx)]
+            come(block, moe_x, (slot(i, dx), o))
+            relay_c[i, dx].append(to(block, block, moe_xc, (i * nx + dx, o), me, mate))
 
     def spread(i, dx):
         n = i * nx + dx
@@ -561,12 +620,8 @@
         for copy in loads[3:]:
             copy.wait()
 
-    def scoped(name, f, *a):
-        with S(name):
-            f(*a)
-
-    def each(name, f, i):
-        for dx in range(nx):
+    def each(name, f, i, some=range(nx)):
+        for dx in some:
             scoped("%s%d%d" % (name, i, dx), f, i, dx)
 
     def half_up(c, k):
@@ -575,59 +630,69 @@
                 scoped("up%d_%d" % (c, f), up, c, f)
 
     last = nz - 1
-    scoped("x_arrive", x_arrive)
+    each("gone", gone, 0, side)
+    for i in range(1, min(3, nz)):
+        each("send", send, i, side)
+    for i in range(3, nz):
+        send(i, 0)
+    each("arrive", arrive, 0, side)
+    scoped("weights", weights_in)
     if nz > 1:
-        each("spread", spread, 1)
-    scoped("weights", weights_in)
-    lat_next = 0
-    for c in range(nz):
+        each("arrive", arrive, 1, range(1))
+    scoped("finish0", finish, 0)
+    half_up(0, 0)
+    for i in range(3, nz):
+        each("send", send, i, side)
+    half_up(0, 1)
+    scoped("down0", down, 0)
+    if nz > 1:
+        each("spread", spread, 1, side)
+        scoped("level_two0", level_two, 0)
+        each("forward", forward, 1, side)
+        scoped("finish1", finish, 1)
+        half_up(1, 0)
+    scoped("lat0", lat_hop, 0)
+    if nz > 2:
+        each("spread", spread, 2)
+    if nz > 1:
+        half_up(1, 1)
+    for i in range(3, nz):
+        each("spread", spread, i)
+    if nz > 1:
+        scoped("down1", down, 1)
+        scoped("lat1", lat_hop, 1)
+        if nz > 2:
+            each("forward", forward, 2)
+        scoped("level_two1", level_two, 1)
+        scoped("give_back0", give_back, 0)
+    for c in range(2, nz):
         scoped("finish%d" % c, finish, c)
         half_up(c, 0)
-        if c == 0 and nz > 1:
-            scoped("forward10", forward, 1, 0)
-        if 1 <= c and 2 < c + 1 < nz + 0:
-            scoped("spread%d0" % (c + 1), spread, c + 1, 0)
+        if c + 1 < nz:
+            each("forward", forward, c + 1, range(1))
+        scoped("lat%d" % c, lat_hop, c)
         half_up(c, 1)
-        if 1 <= c and 2 < c + 1 < nz + 0:
-            for dx in range(1, nx):
-                scoped("spread%d%d" % (c + 1, dx), spread, c + 1, dx)
-        if c > 0:
-            scoped("level_two%d" % (c - 1), level_two, c - 1)
+        if c + 1 < nz:
+            each("forward", forward, c + 1, side)
         scoped("down%d" % c, down, c)
-        if c == 0 and nz > 1:
-            for dx in range(1, nx):
-                scoped("forward1%d" % dx, forward, 1, dx)
-        if 1 <= c and 2 < c + 1 < nz + 0:
-            each("forward", forward, c + 1)
-        if c == 0 and nz > 2:
-            each("spread", spread, 2)
-            each("forward", forward, 2)
-        if c > 0:
-            scoped("give_back%d" % (c - 1), give_back, c - 1)
-            scoped("lat%d" % lat_next, lat_hop, lat_next)
-            lat_next += 1
-    scoped("level_two%d" % last, level_two, last)
-    while lat_next < nz:
-        scoped("lat%d" % lat_next, lat_hop, lat_next)
-        lat_next += 1
-    scoped("give_back%d" % last, give_back, last)
-    each("combine", combine, 0)
+        scoped("level_two%d" % c, level_two, c)
+        scoped("give_back%d" % (c - 1), give_back, c - 1)
     for z in range(nz):
         scoped("cross%d" % z, lat_cross, z)
+    each("combine", combine, 0)
     for z in range(nz):
         scoped("lat_done%d" % z, lat_done, z)
     with S("expand"):
         lax.fori_loop(0, g_lat.shape[0], expand, 0)
+    scoped("give_back%d" % last, give_back, last)
     for p in range(parts):
         scoped("attend%d" % p, attend, p)
         att_send(p)
-    for i in range(1, nz - 1):
-        each("combine", combine, i)
     for p in range(parts):
         scoped("att_forward%d" % p, att_forward, p)
     scoped("project", project)
-    if nz > 1:
-        each("combine", combine, last)
+    for i in range(1, nz):
+        each("combine", combine, i)
     for copy in sends:
         copy.wait_send()
     lat_drain()
@@ -669,6 +734,7 @@
         wo = wo.reshape(n_tp * heads * LANES, out_proj.shape[1])
         parts = heads
     model_width = moe_input.shape[1]
+    top = routes.shape[1]
     capacity = 3 * row_count // n_ep
     places = -(-capacity // 16) * 16
     columns = model_width // n_tp
@@ -679,12 +745,17 @@
     attention, experts = pl.pallas_call(
         functools.partial(fused, n_ep, n_tp, heads, (PLAIN_HEAD_DIM + ROPE) ** (-0.5)),
         out_shape=(
-            jax.ShapeDtypeStruct((row_count, out_proj.shape[1]), jnp.float32),
-            jax.ShapeDtypeStruct((row_count, columns), jnp.float32),
+            pltpu.VMEM((row_count, out_proj.shape[1]), jnp.float32),
+            pltpu.VMEM((row_count, columns), jnp.float32),
         ),
-        in_specs=[vmem] * 5 + [hbm] * 8,
+        in_specs=[hbm] * 13,
         out_specs=(vmem, vmem),
         scratch_shapes=[
+            pltpu.VMEM((top, row_count), jnp.int32),
+            pltpu.VMEM((top, row_count), jnp.float32),
+            pltpu.VMEM((1, model_width), jnp.float32),
+            pltpu.VMEM((1, latent), jnp.float32),
+            pltpu.VMEM((ROPE, row_count), bf16),
             pltpu.VMEM((row_count, model_width), bf16),
             pltpu.VMEM((share, latent), bf16),
             pltpu.VMEM(queries.shape, bf16),
@@ -697,7 +768,7 @@
             pltpu.VMEM((n_ep, row_count), jnp.int32),
             pltpu.VMEM((n_ep, row_count), jnp.float32),
             pltpu.VMEM((n_ep, places, columns), bf16),
-            pltpu.VMEM((nx, n_y, places, columns), bf16),
+            pltpu.VMEM((min(2, nz) * nx, n_y, places, columns), bf16),
             pltpu.VMEM((LANES, row_count), jnp.float32),
             pltpu.VMEM((row_count, heads * LANES), bf16),
             pltpu.VMEM((CORES * nx, nz, share, latent + LANES), bf16),
@@ -711,14 +782,14 @@
             pltpu.VMEM((n_y, nz, nx, places, columns), bf16),
             pltpu.VMEM((n_ep, places, columns), bf16),
             pltpu.VMEM((n_ep, places, columns), bf16),
-            pltpu.SemaphoreType.DMA((8,)),
+            pltpu.SemaphoreType.DMA((13,)),
             dma(nz),
             dma(nz),
             dma(nz),
             dma(nx, nz),
             dma(n_ep),
-            dma(nx, n_y),
-            dma(nx, n_y),
+            dma(n_ep, n_y),
+            dma(n_ep, n_y),
             dma(n_y, n_ep),
             dma(n_y, n_ep),
             dma(n_y, parts),
@@ -728,7 +799,7 @@
             dma(n_ep),
         ],
         compiler_params=pltpu.CompilerParams(
-            collective_id=0, has_side_effects=True, vmem_limit_bytes=50 * 1024 * 1024
+            collective_id=0, has_side_effects=True, vmem_limit_bytes=60 * 1024 * 1024
         ),
         name="fused",
     )(

time: 84.8 us -> 66.5 us (0.78)
  Pallas kernels: 74.7 us -> 64.2 us
  local copies, waits for them, and re-layouts: 7.59 us -> 0 us
    pallas_call x1, Pallas kernels: 74.7 us -> 64.2 us  [local(): pl.pallas_call(functools.partial(fused, n_ep, n_tp, heads, (PLAIN_HEAD_DI...]
    unnamed x18 -> x0, local copies, waits for them, and re-layouts: 7.59 us -> none
where the time goes in v2:
time: 66.5 us; the launch traced here: 66.3 us
  Pallas kernels  64.2 us (97%)
  other arithmetic  1.47 us (2%)
    pallas_call x1, Pallas kernels, local(): pl.pallas_call(functools.partial(fused, n_ep, n_tp, heads, (PLAIN_HEAD_DI...  64.2 us
    convert_element_type x2, other arithmetic, local(): return (attention.astype(bf16), experts.astype(bf16))  1.47 us

profile of v2, /device:TPU:0, one launch (start us, length us, event | category | flops | bytes accessed | tf_op | source)
XLA Modules:
  0.0 66.3 jit_solution(13667201017350922291)
XLA Ops:
  0.6 64.2 %fused.1 = (f32[256,512]{1,0:T(8,128)S(1)}, f32[256,512]{1,0:T(8,128)S(1)}) custom-call(s32[2,256]{1,0:T(2,128)} %bitcast.13, f32[2,256]{1,0:T(2,128)} %bitcast.14, f32[1,2048]{1,0:T(1,128)} %bitcast.12, f32[1,512]{1,0:T(1,128)} %bitcast.15, bf16[32,256]{1,0:T(8,128)(2,1)} %bitcast.11, bf16[256,2048]{1,0:T(8,128)(2,1)} %moe_hbm.1, bf16[256,512]{1,0:T(8,128)(2,1)} %ckv_hbm.1, ...), custom_call_target="tpu_custom_call" | custom-call | tf_op jit(solution)/shard_map/fused/pallas_call | solution.py:745
  64.9 0.7 %convert_element_type.6 = bf16[256,512]{1,0:T(8,128)(2,1)} convert(f32[256,512]{1,0:T(8,128)S(1)} %get-tuple-element.4) | non-fusion elementwise | flops 131072 | bytes 786432 | tf_op jit(solution)/shard_map/convert_element_type | solution.py:820
  65.6 0.7 %convert_element_type.7 = bf16[256,512]{1,0:T(8,128)(2,1)} convert(f32[256,512]{1,0:T(8,128)S(1)} %get-tuple-element.5) | non-fusion elementwise | flops 131072 | bytes 786432 | tf_op jit(solution)/shard_map/convert_element_type | solution.py:820

commit v3 on v2

--- a/solution.py
+++ b/solution.py
@@ -57,8 +57,8 @@
     wg_hbm,
     wu_hbm,
     wd_hbm,
-    att_out,
-    exp_out,
+    att_dst,
+    exp_dst,
     routes_ref,
     weight_ref,
     mgain_ref,
@@ -90,6 +90,9 @@
     r2,
     tot,
     back,
+    acc,
+    att_v,
+    exp_v,
     in_sem,
     lat_up,
     lat_dn,
@@ -265,7 +268,7 @@
 
 
     def direct(i, dx):
-        return i == 0 or (i == 1 and dx == 0)
+        return i == 0
 
     sent = {}
 
@@ -285,10 +288,10 @@
                     out_x.at[n, o],
                     g_moe.at[o * CORES + my_c, seen(dx)],
                     moe_x,
-                    (n, o),
+                    (dx - 1, o),
                     at(i, dx),
                     tp,
-                    (seen(dx), o),
+                    (nx - dx - 1, o),
                 )
                 for o in range(n_y)
             ]
@@ -303,27 +306,26 @@
             sends[:] = [other for other in sends if other is not copy]
 
     side = range(1, nx)
+    wave = [(0, dx) for dx in side] + [(i, 0) for i in range(1, nz)]
+    later = [(i, dx) for i in range(1, nz) for dx in side]
     with S("gather_a"):
-        for dx in side:
-            gather(0, dx)
-        if nz > 1:
-            gather(1, 0)
-        if nz > 2:
-            gather(2, 0)
+        for pair in wave[:2]:
+            gather(*pair)
     with S("barrier"):
         pl.semaphore_wait(barrier, n_ep + n_tp - 2)
-    for dx in side:
-        send(0, dx)
-    for i in range(1, min(3, nz)):
-        send(i, 0)
+    for pair in wave[:2]:
+        send(*pair)
     with S("gather_b"):
-        for i in range(1, nz):
-            for dx in range(nx):
-                if dx or i > 2:
-                    gather(i, dx)
+        for pair in wave[2:]:
+            gather(*pair)
+            send(*pair)
     with S("gather_own"):
         for t in range(n_tp):
             g_moe[t, slot(0, 0)] = rows_for(me, slice(t * columns, (t + 1) * columns))
+    with S("gather_c"):
+        for pair in later:
+            gather(*pair)
+            send(*pair)
 
     with S("prep"):
         half = ROPE // 2
@@ -454,80 +456,114 @@
         relay_c[i, dx] = []
         for o in range(n_y):
             block = g_moe.at[o * CORES + my_c, slot(i, dx)]
-            come(block, moe_x, (slot(i, dx), o))
-            relay_c[i, dx].append(to(block, block, moe_xc, (i * nx + dx, o), me, mate))
-
-    def spread(i, dx):
+            come(block, moe_x, (dx - 1, o))
+            relay_c[i, dx].append(to(block, block, moe_xc, (dx - 1, o), me, mate))
+
+    def spread(i, dx, when=None):
         n = i * nx + dx
         block = g_moe.at[tp, slot(i, dx)]
-        come(block, moe_a, (slot(i, dx),))
+        copies = []
         for o in range(1, n_y):
             other = lax.rem(my_y + o, n_y) * CORES + my_c
-            relay_y[n, o] = to(block, block, moe_y, (o, n), me, other)
-        relay_c[i, dx] = [to(block, block, moe_c, (0, n), me, mate)]
+            relay_y[n, o] = remote(block, block, moe_y, (o - 1, n - nx), (o - 1, n - nx), me, other)
+            copies.append(relay_y[n, o])
+        relay_c[i, dx] = [remote(block, block, moe_c, (0, n - nx), (0, n - nx), me, mate)]
+        copies += relay_c[i, dx]
+
+        def run():
+            come(block, moe_a, (slot(i, dx),))
+            for copy in copies:
+                copy.start()
+
+        if when is None:
+            run()
+            sends.extend(copies)
+        else:
+            pl.when(when)(run)
+            if (i, dx) not in spread_once:
+                spread_once.add((i, dx))
+                sends.extend(copies)
+
+    spread_once = set()
+    inner = jnp.logical_and(my_z > 0, my_z + 1 < nz)
+    outer = jnp.logical_not(inner)
 
     def forward(i, dx):
         n = i * nx + dx
         for o in range(1, n_y):
             relay_y[n, o].wait_recv()
             came = g_moe.at[lax.rem(my_y + n_y - o, n_y) * CORES + my_c, slot(i, dx)]
-            relay_c[i, dx].append(to(came, came, moe_c, (o, n), me, mate))
+            relay_c[i, dx].append(to(came, came, moe_c, (o, n - nx), me, mate))
 
     def finish(i):
         for dx in range(nx):
             for copy in relay_c.get((i, dx), ()):
                 copy.wait_recv()
 
-    def up(c, f):
+    units = [(0, (dx,)) for dx in range(nx)] + [(c, tuple(range(nx))) for c in range(1, nz)]
+
+    def up(u, f):
+        c, dxs = units[u]
         span = slice(f * tile, (f + 1) * tile)
+        rows = len(dxs) * cap
         gate = jnp.zeros((rows, tile), f32)
         lift = jnp.zeros((rows, tile), f32)
         for t in range(n_tp):
-            x = merge_rows(g_moe[t, pl.ds(zs[c] * nx, nx)])
+            x = merge_rows(g_moe[t, pl.ds(slot(c, dxs[0]), len(dxs))])
             gate += jnp.dot(
                 x, wg[t * columns : (t + 1) * columns, span], preferred_element_type=f32
             )
             lift += jnp.dot(
                 x, wu[t * columns : (t + 1) * columns, span], preferred_element_type=f32
             )
-        hidden[:, span] = (gate / (1.0 + jnp.exp(-gate)) * lift).astype(bf16)
+        hidden[:rows, span] = (gate / (1.0 + jnp.exp(-gate)) * lift).astype(bf16)
 
     reduce_c, reduce_y = {}, {}
 
-    def down(c):
+    def down(u):
+        c, dxs = units[u]
+        n = c * nx + dxs[0]
+        group = slice(n, n + len(dxs))
+        span = pl.ds(n, len(dxs))
         for o in list(range(1, n_y)) + [0]:
             y = lax.rem(my_y + o, n_y)
             for mine in range(2):
                 t = y * CORES + (my_c if mine else 1 - my_c)
-                part[t, c] = (
-                    jnp.dot(hidden[...], wd[:, lane_block(t)], preferred_element_type=f32)
+                part[t, group] = (
+                    jnp.dot(
+                        hidden[: len(dxs) * cap],
+                        wd[:, lane_block(t)],
+                        preferred_element_type=f32,
+                    )
                     .astype(bf16)
-                    .reshape(nx, cap, columns)
+                    .reshape(len(dxs), cap, columns)
                 )
                 if not mine:
-                    reduce_c[c, o] = to(part.at[t, c], r1.at[o, c], red_c, (o, c), me, mate)
-
-    def level_two(c):
+                    reduce_c[u, o] = to(part.at[t, span], r1.at[o, span], red_c, (o, u), me, mate)
+
+    def level_two(u):
+        c, dxs = units[u]
         for o in range(1, n_y):
             y = lax.rem(my_y + o, n_y)
-            reduce_c[c, o].wait_recv()
-            for dx in range(nx):
+            reduce_c[u, o].wait_recv()
+            for dx in dxs:
                 n = c * nx + dx
-                s2[o, c, dx] = (
-                    part[y * CORES + my_c, c, dx].astype(f32) + r1[o, c, dx].astype(f32)
+                s2[o, n] = (
+                    part[y * CORES + my_c, n].astype(f32) + r1[o, n].astype(f32)
                 ).astype(bf16)
                 reduce_y[n, o] = to(
-                    s2.at[o, c, dx], r2.at[o, c, dx], red_y, (o, n), me, y * CORES + my_c
+                    s2.at[o, n], r2.at[o, n], red_y, (o - 1, n), me, y * CORES + my_c
                 )
 
-    def give_back(c):
-        reduce_c[c, 0].wait_recv()
-        for dx in range(nx):
+    def give_back(u):
+        c, dxs = units[u]
+        reduce_c[u, 0].wait_recv()
+        for dx in dxs:
             n = c * nx + dx
-            total = part[tp, c, dx].astype(f32) + r1[0, c, dx].astype(f32)
+            total = part[tp, n].astype(f32) + r1[0, n].astype(f32)
             for o in range(1, n_y):
                 reduce_y[n, o].wait_recv()
-                total += r2[o, c, dx].astype(f32)
+                total += r2[o, n].astype(f32)
             tot[n] = total.astype(bf16)
             if n > 0:
                 to(tot.at[n], back.at[seen(dx)], ret_a, (n,), at(c, dx), tp, (seen(dx),))
@@ -549,9 +585,9 @@
             preferred_element_type=f32,
         )
         if i == 0 and dx == 0:
-            exp_out[...] = add
+            acc[...] = add
         else:
-            exp_out[...] += add
+            acc[...] += add
 
     block = nz * share
 
@@ -596,7 +632,7 @@
         own = g_att.at[tp, p]
         for o in range(1, n_y):
             other = lax.rem(my_y + o, n_y) * CORES + my_c
-            att_in.append((p, o, to(own, own, att_y, (o, p), me, other)))
+            att_in.append((p, o, to(own, own, att_y, (o - 1, p), me, other)))
         att_mate.append(to(own, own, att_c, (0, p), me, mate))
 
     def att_forward(part_index):
@@ -606,15 +642,19 @@
                 came = g_att.at[lax.rem(my_y + n_y - o, n_y) * CORES + my_c, p]
                 att_mate.append(to(came, came, att_c, (o, p), me, mate))
 
+    att_copy = pltpu.make_async_copy(att_v, att_dst, in_sem.at[13])
+    exp_copy = pltpu.make_async_copy(exp_v, exp_dst, in_sem.at[14])
+
     def project():
         for copy in att_mate:
             copy.wait_recv()
-        total = jnp.zeros(att_out.shape, f32)
+        total = jnp.zeros(att_v.shape, f32)
         for t in range(n_tp):
             x = jnp.concatenate([g_att[t, p] for p in range(g_att.shape[1])], axis=1)
             width = x.shape[1]
             total += jnp.dot(x, wo_ref[t * width : (t + 1) * width, :], preferred_element_type=f32)
-        att_out[...] = total
+        att_v[...] = total.astype(bf16)
+        att_copy.start()
 
     def weights_in():
         for copy in loads[3:]:
@@ -624,59 +664,75 @@
         for dx in some:
             scoped("%s%d%d" % (name, i, dx), f, i, dx)
 
-    def half_up(c, k):
+    def half_up(u, k):
         for f in range(tiles):
             if (2 * f) // tiles == k:
-                scoped("up%d_%d" % (c, f), up, c, f)
+                scoped("up%d_%d" % (u, f), up, u, f)
 
     last = nz - 1
-    each("gone", gone, 0, side)
-    for i in range(1, min(3, nz)):
-        each("send", send, i, side)
-    for i in range(3, nz):
-        send(i, 0)
-    each("arrive", arrive, 0, side)
+    first = nx - 1
     scoped("weights", weights_in)
+    half_up(0, 0)
     if nz > 1:
-        each("arrive", arrive, 1, range(1))
-    scoped("finish0", finish, 0)
-    half_up(0, 0)
-    for i in range(3, nz):
-        each("send", send, i, side)
+        each("spread", spread, 1, range(1))
     half_up(0, 1)
     scoped("down0", down, 0)
+    each("arrive", arrive, 0, side)
+    scoped("level_two0", level_two, 0)
+    scoped("finish0", finish, 0)
+    for u in range(1, nx):
+        half_up(u, 0)
+        if nz > 1 and u == 1:
+            each("spread", spread, 1, side)
+        half_up(u, 1)
+        scoped("down%d" % u, down, u)
     if nz > 1:
-        each("spread", spread, 1, side)
-        scoped("level_two0", level_two, 0)
+        each("forward", forward, 1, range(1))
+    if nz > 2:
+        for dx in range(nx):
+            scoped("ispread2%d" % dx, spread, 2, dx, inner)
+    for u in range(1, nx):
+        scoped("level_two%d" % u, level_two, u)
+    scoped("lat0", lat_hop, 0)
+    if nz > 1:
         each("forward", forward, 1, side)
         scoped("finish1", finish, 1)
-        half_up(1, 0)
-    scoped("lat0", lat_hop, 0)
+        half_up(first + 1, 0)
     if nz > 2:
-        each("spread", spread, 2)
-    if nz > 1:
-        half_up(1, 1)
+        for dx in range(nx):
+            scoped("ospread2%d" % dx, spread, 2, dx, outer)
     for i in range(3, nz):
         each("spread", spread, i)
     if nz > 1:
-        scoped("down1", down, 1)
+        half_up(first + 1, 1)
+        scoped("down%d" % (first + 1), down, first + 1)
         scoped("lat1", lat_hop, 1)
         if nz > 2:
             each("forward", forward, 2)
-        scoped("level_two1", level_two, 1)
-        scoped("give_back0", give_back, 0)
     for c in range(2, nz):
+        u = first + c
         scoped("finish%d" % c, finish, c)
-        half_up(c, 0)
+        scoped("level_two%d" % (u - 1), level_two, u - 1)
+        half_up(u, 0)
         if c + 1 < nz:
             each("forward", forward, c + 1, range(1))
+        if c == 2:
+            for v in range(nx):
+                scoped("give_back%d" % v, give_back, v)
+        else:
+            scoped("give_back%d" % (u - 2), give_back, u - 2)
         scoped("lat%d" % c, lat_hop, c)
-        half_up(c, 1)
+        half_up(u, 1)
         if c + 1 < nz:
             each("forward", forward, c + 1, side)
-        scoped("down%d" % c, down, c)
-        scoped("level_two%d" % c, level_two, c)
-        scoped("give_back%d" % (c - 1), give_back, c - 1)
+        scoped("down%d" % u, down, u)
+    final = len(units) - 1
+    scoped("level_two%d" % final, level_two, final)
+    if nz > 1:
+        scoped("give_back%d" % (final - 1), give_back, final - 1)
+    if nz == 2:
+        for v in range(nx):
+            scoped("give_back%d" % v, give_back, v)
     for z in range(nz):
         scoped("cross%d" % z, lat_cross, z)
     each("combine", combine, 0)
@@ -684,18 +740,26 @@
         scoped("lat_done%d" % z, lat_done, z)
     with S("expand"):
         lax.fori_loop(0, g_lat.shape[0], expand, 0)
-    scoped("give_back%d" % last, give_back, last)
     for p in range(parts):
         scoped("attend%d" % p, attend, p)
         att_send(p)
+        if p == 0:
+            scoped("give_back%d" % final, give_back, final)
     for p in range(parts):
         scoped("att_forward%d" % p, att_forward, p)
     scoped("project", project)
     for i in range(1, nz):
         each("combine", combine, i)
-    for copy in sends:
-        copy.wait_send()
-    lat_drain()
+    exp_v[...] = acc[...].astype(bf16)
+    exp_copy.start()
+    with S("sendwait"):
+        for copy in sends:
+            copy.wait_send()
+    with S("latdrain"):
+        lat_drain()
+    with S("outwait"):
+        att_copy.wait()
+        exp_copy.wait()
 
 
 def local(
@@ -739,17 +803,17 @@
     places = -(-capacity // 16) * 16
     columns = model_width // n_tp
     ff = gate_weight.shape[2]
-    vmem = pl.BlockSpec(memory_space=pltpu.VMEM)
+    anywhere = pl.BlockSpec(memory_space=pl.ANY)
     hbm = pl.BlockSpec(memory_space=pltpu.HBM)
     dma = lambda *shape: pltpu.SemaphoreType.DMA((2,) + shape)
     attention, experts = pl.pallas_call(
         functools.partial(fused, n_ep, n_tp, heads, (PLAIN_HEAD_DIM + ROPE) ** (-0.5)),
         out_shape=(
-            pltpu.VMEM((row_count, out_proj.shape[1]), jnp.float32),
-            pltpu.VMEM((row_count, columns), jnp.float32),
+            pltpu.VMEM((row_count, out_proj.shape[1]), bf16),
+            pltpu.VMEM((row_count, columns), bf16),
         ),
         in_specs=[hbm] * 13,
-        out_specs=(vmem, vmem),
+        out_specs=(anywhere, anywhere),
         scratch_shapes=[
             pltpu.VMEM((top, row_count), jnp.int32),
             pltpu.VMEM((top, row_count), jnp.float32),
@@ -768,7 +832,7 @@
             pltpu.VMEM((n_ep, row_count), jnp.int32),
             pltpu.VMEM((n_ep, row_count), jnp.float32),
             pltpu.VMEM((n_ep, places, columns), bf16),
-            pltpu.VMEM((min(2, nz) * nx, n_y, places, columns), bf16),
+            pltpu.VMEM((nx, n_y, places, columns), bf16),
             pltpu.VMEM((LANES, row_count), jnp.float32),
             pltpu.VMEM((row_count, heads * LANES), bf16),
             pltpu.VMEM((CORES * nx, nz, share, latent + LANES), bf16),
@@ -776,26 +840,29 @@
             pltpu.VMEM((n_tp, parts, row_count, LANES), bf16),
             pltpu.VMEM((n_ep * row_count, heads * LANES), bf16),
             pltpu.VMEM((nx * places, ff), bf16),
-            pltpu.VMEM((n_tp, nz, nx, places, columns), bf16),
-            pltpu.VMEM((n_y, nz, nx, places, columns), bf16),
-            pltpu.VMEM((n_y, nz, nx, places, columns), bf16),
-            pltpu.VMEM((n_y, nz, nx, places, columns), bf16),
+            pltpu.VMEM((n_tp, n_ep, places, columns), bf16),
+            pltpu.VMEM((n_y, n_ep, places, columns), bf16),
+            pltpu.VMEM((n_y, n_ep, places, columns), bf16),
+            pltpu.VMEM((n_y, n_ep, places, columns), bf16),
             pltpu.VMEM((n_ep, places, columns), bf16),
             pltpu.VMEM((n_ep, places, columns), bf16),
-            pltpu.SemaphoreType.DMA((13,)),
+            pltpu.VMEM((row_count, columns), jnp.float32),
+            pltpu.VMEM((row_count, out_proj.shape[1]), bf16),
+            pltpu.VMEM((row_count, columns), bf16),
+            pltpu.SemaphoreType.DMA((15,)),
             dma(nz),
             dma(nz),
             dma(nz),
             dma(nx, nz),
             dma(n_ep),
-            dma(n_ep, n_y),
-            dma(n_ep, n_y),
-            dma(n_y, n_ep),
-            dma(n_y, n_ep),
+            dma(max(nx - 1, 1), n_y),
+            dma(max(nx - 1, 1), n_y),
+            dma(max(n_y - 1, 1), max(n_ep - nx, 1)),
+            dma(n_y, max(n_ep - nx, 1)),
+            dma(max(n_y - 1, 1), parts),
             dma(n_y, parts),
-            dma(n_y, parts),
-            dma(n_y, nz),
-            dma(n_y, n_ep),
+            dma(n_y, nx + nz - 1),
+            dma(max(n_y - 1, 1), n_ep),
             dma(n_ep),
         ],
         compiler_params=pltpu.CompilerParams(
@@ -817,7 +884,7 @@
         up_weight.reshape(model_width, ff),
         down_weight.reshape(ff, model_width),
     )
-    return attention.astype(bf16), experts.astype(bf16)
+    return attention, experts
 
 
 def solution(mesh):

time: 66.5 us -> 66.5 us (level)
  other arithmetic: 1.47 us -> 0 us
  local copies, waits for them, and re-layouts: 0 us -> 1.41 us
    convert_element_type x2 -> x0, other arithmetic: 1.47 us -> none  [local(): return (attention.astype(bf16), experts.astype(bf16))]
    unnamed x0 -> x2, local copies, waits for them, and re-layouts: none -> 1.41 us
where the time goes in v3:
time: 66.5 us; the launch traced here: 66.3 us
  Pallas kernels  64.3 us (97%)
  local copies, waits for them, and re-layouts  1.41 us (2%)
    pallas_call x1, Pallas kernels, local(): pl.pallas_call(functools.partial(fused, n_ep, n_tp, heads, (PLAIN_HEAD_DI...  64.3 us
    unnamed x2, local copies, waits for them, and re-layouts  1.41 us

profile of v3, /device:TPU:0, one launch (start us, length us, event | category | flops | bytes accessed | tf_op | source)
XLA Modules:
  0.0 66.3 jit_solution(145095919770204227)
XLA Ops:
  0.6 64.3 %fused.1 = (bf16[256,512]{1,0:T(8,128)(2,1)S(1)}, bf16[256,512]{1,0:T(8,128)(2,1)S(1)}) custom-call(s32[2,256]{1,0:T(2,128)} %bitcast.13, f32[2,256]{1,0:T(2,128)} %bitcast.14, f32[1,2048]{1,0:T(1,128)} %bitcast.12, f32[1,512]{1,0:T(1,128)} %bitcast.15, bf16[32,256]{1,0:T(8,128)(2,1)} %bitcast.11, bf16[256,2048]{1,0:T(8,128)(2,1)} %moe_hbm.1, ...), custom_call_target="tpu_custom_call" | custom-call | tf_op jit(solution)/shard_map/fused/pallas_call | solution.py:809
  64.9 0.7 %copy.17 = bf16[256,512]{1,0:T(8,128)(2,1)} copy(bf16[256,512]{1,0:T(8,128)(2,1)S(1)} %get-tuple-element.2) | data formatting | bytes 524288
  65.6 0.7 %copy.18 = bf16[256,512]{1,0:T(8,128)(2,1)} copy(bf16[256,512]{1,0:T(8,128)(2,1)S(1)} %get-tuple-element.3) | data formatting | bytes 524288

commit v4 on v3

--- a/solution.py
+++ b/solution.py
@@ -126,7 +126,7 @@
     chunks = nz
     rows = nx * cap
     ff = wg.shape[1]
-    tile = min(256, ff)
+    tile = min(512, ff)
     tiles = ff // tile
     share = ckv_v.shape[0]
     latent = ckv_v.shape[1]
@@ -170,7 +170,16 @@
     def lane_block(t):
         return pl.ds(pl.multiple_of(t * columns, columns), columns)
 
-    S = jax.named_scope
+    class S:
+        def __init__(self, name):
+            self.scope = jax.named_scope(name)
+
+        def __enter__(self):
+            pl.delay(1)
+            self.scope.__enter__()
+
+        def __exit__(self, *args):
+            self.scope.__exit__(*args)
 
     def scoped(name, f, *a):
         with S(name):
@@ -306,8 +315,9 @@
             sends[:] = [other for other in sends if other is not copy]
 
     side = range(1, nx)
-    wave = [(0, dx) for dx in side] + [(i, 0) for i in range(1, nz)]
-    later = [(i, dx) for i in range(1, nz) for dx in side]
+    wave = [(0, dx) for dx in side] + [(i, 0) for i in range(1, min(3, nz))]
+    later = [(i, dx) for i in (2, 1) for dx in side if i < nz]
+    latest = [(i, dx) for i in range(3, nz) for dx in range(nx)]
     with S("gather_a"):
         for pair in wave[:2]:
             gather(*pair)
@@ -326,6 +336,8 @@
         for pair in later:
             gather(*pair)
             send(*pair)
+        for pair in latest:
+            gather(*pair)
 
     with S("prep"):
         half = ROPE // 2
@@ -591,11 +603,20 @@
 
     block = nz * share
 
-    def expand(t, carry):
-        kv[pl.ds(pl.multiple_of(t * block, block), block), :] = jnp.dot(
-            merge_rows(g_lat[t])[:, :latent], wkv_ref[...], preferred_element_type=f32
-        ).astype(bf16)
-        return carry
+    def expand(z):
+        lat_done(z)
+        for t in range(g_lat.shape[0]):
+            span = pl.ds(pl.multiple_of(t * block + z * share, share), share)
+            kv[span, :] = jnp.dot(
+                g_lat[t, z][:, :latent], wkv_ref[...], preferred_element_type=f32
+            ).astype(bf16)
+
+    def around(d, f):
+        if d == 0:
+            f(my_z)
+        else:
+            pl.when(my_z >= d)(lambda: f(my_z - d))
+            pl.when(my_z + d < nz)(lambda: f(my_z + d))
 
     whole_lat = g_lat.reshape(g_lat.shape[0] * block, g_lat.shape[3])
     lane = lax.broadcasted_iota(jnp.int32, (1, LANES), 1)
@@ -665,13 +686,16 @@
             scoped("%s%d%d" % (name, i, dx), f, i, dx)
 
     def half_up(u, k):
-        for f in range(tiles):
-            if (2 * f) // tiles == k:
-                scoped("up%d_%d" % (u, f), up, u, f)
+        with S("up%d_%d" % (u, k)):
+            for f in range(tiles):
+                if (2 * f) // tiles == k:
+                    up(u, f)
 
     last = nz - 1
     first = nx - 1
     scoped("weights", weights_in)
+    for pair in latest:
+        send(*pair)
     half_up(0, 0)
     if nz > 1:
         each("spread", spread, 1, range(1))
@@ -683,17 +707,23 @@
     for u in range(1, nx):
         half_up(u, 0)
         if nz > 1 and u == 1:
-            each("spread", spread, 1, side)
+            for dx in side:
+                scoped("ospread1%d" % dx, spread, 1, dx, outer)
         half_up(u, 1)
         scoped("down%d" % u, down, u)
     if nz > 1:
+        for dx in side:
+            scoped("ispread1%d" % dx, spread, 1, dx, inner)
+    if nz > 2:
+        scoped("ispread20", spread, 2, 0, inner)
+    if nz > 1:
         each("forward", forward, 1, range(1))
-    if nz > 2:
-        for dx in range(nx):
-            scoped("ispread2%d" % dx, spread, 2, dx, inner)
     for u in range(1, nx):
         scoped("level_two%d" % u, level_two, u)
     scoped("lat0", lat_hop, 0)
+    if nz > 2:
+        for dx in side:
+            scoped("ispread2%d" % dx, spread, 2, dx, inner)
     if nz > 1:
         each("forward", forward, 1, side)
         scoped("finish1", finish, 1)
@@ -733,18 +763,25 @@
     if nz == 2:
         for v in range(nx):
             scoped("give_back%d" % v, give_back, v)
-    for z in range(nz):
-        scoped("cross%d" % z, lat_cross, z)
+    for d in range(min(2, nz)):
+        scoped("cross%d" % d, around, d, lat_cross)
+    scoped("expand0", around, 0, expand)
+    for d in range(2, nz):
+        if d == last:
+            scoped("expand%d" % (d - 2), around, d - 2, expand)
+            scoped("expand%d" % (d - 1), around, d - 1, expand)
+            scoped("cross%d" % d, around, d, lat_cross)
+        else:
+            scoped("cross%d" % d, around, d, lat_cross)
+            if d > 2:
+                scoped("expand%d" % (d - 2), around, d - 2, expand)
     each("combine", combine, 0)
-    for z in range(nz):
-        scoped("lat_done%d" % z, lat_done, z)
-    with S("expand"):
-        lax.fori_loop(0, g_lat.shape[0], expand, 0)
+    if nz > 1:
+        scoped("expand%d" % last, around, last, expand)
+    scoped("give_back%d" % final, give_back, final)
     for p in range(parts):
         scoped("attend%d" % p, attend, p)
         att_send(p)
-        if p == 0:
-            scoped("give_back%d" % final, give_back, final)
     for p in range(parts):
         scoped("att_forward%d" % p, att_forward, p)
     scoped("project", project)

time: 66.5 us -> 63.4 us (0.953)
  Pallas kernels: 64.3 us -> 61.1 us
    pallas_call x1, Pallas kernels: 64.3 us -> 61.1 us  [local(): pl.pallas_call(functools.partial(fused, n_ep, n_tp, heads, (PLAIN_HEAD_DI...]
where the time goes in v4:
time: 63.4 us; the launch traced here: 63.2 us
  Pallas kernels  61.1 us (96%)
  local copies, waits for them, and re-layouts  1.41 us (2%)
  between operations  0.64 us (1%)
    pallas_call x1, Pallas kernels, local(): pl.pallas_call(functools.partial(fused, n_ep, n_tp, heads, (PLAIN_HEAD_DI...  61.1 us
    unnamed x2, local copies, waits for them, and re-layouts  1.41 us

profile of v4, /device:TPU:0, one launch (start us, length us, event | category | flops | bytes accessed | tf_op | source)
XLA Modules:
  0.0 63.2 jit_solution(6434923196056519789)
XLA Ops:
  0.6 61.1 %fused.1 = (bf16[256,512]{1,0:T(8,128)(2,1)S(1)}, bf16[256,512]{1,0:T(8,128)(2,1)S(1)}) custom-call(s32[2,256]{1,0:T(2,128)} %bitcast.13, f32[2,256]{1,0:T(2,128)} %bitcast.14, f32[1,2048]{1,0:T(1,128)} %bitcast.12, f32[1,512]{1,0:T(1,128)} %bitcast.15, bf16[32,256]{1,0:T(8,128)(2,1)} %bitcast.11, bf16[256,2048]{1,0:T(8,128)(2,1)} %moe_hbm.1, ...), custom_call_target="tpu_custom_call" | custom-call | tf_op jit(solution)/shard_map/fused/pallas_call | solution.py:846
  61.8 0.7 %copy.17 = bf16[256,512]{1,0:T(8,128)(2,1)} copy(bf16[256,512]{1,0:T(8,128)(2,1)S(1)} %get-tuple-element.2) | data formatting | bytes 524288
  62.5 0.7 %copy.18 = bf16[256,512]{1,0:T(8,128)(2,1)} copy(bf16[256,512]{1,0:T(8,128)(2,1)S(1)} %get-tuple-element.3) | data formatting | bytes 524288

commit v5 on v4

--- a/solution.py
+++ b/solution.py
@@ -94,8 +94,7 @@
     att_v,
     exp_v,
     in_sem,
-    lat_up,
-    lat_dn,
+    lat_z,
     lat_x,
     lat_c,
     moe_a,
@@ -389,17 +388,27 @@
 
     lat_over, lat_side = {}, {}
 
+    def hop(block, way, z, ep_id, tp_id=tp):
+        return pltpu.make_async_remote_copy(
+            src_ref=block,
+            dst_ref=block,
+            send_sem=lat_z.at[way, z],
+            recv_sem=lat_z.at[0, z],
+            device_id=(ep_id, tp_id),
+            device_id_type=pl.DeviceIdType.MESH,
+        )
+
     def lat_hop(d):
         if d == 0:
             src = g_lat.at[own_lat, my_z]
 
             @pl.when(my_z + 1 < nz)
             def _():
-                remote(src, src, lat_up, (my_z,), (my_z,), me + nx, tp).start()
+                hop(src, 1, my_z, me + nx).start()
 
             @pl.when(my_z > 0)
             def _():
-                remote(src, src, lat_dn, (my_z,), (my_z,), me - nx, tp).start()
+                hop(src, 2, my_z, me - nx).start()
 
             lat_share(my_z)
         else:
@@ -407,11 +416,11 @@
             def _():
                 z = my_z - d
                 src = g_lat.at[own_lat, z]
-                come(src, lat_up, (z,))
+                hop(src, 1, z, me, mate).wait_recv()
 
                 @pl.when(my_z + 1 < nz)
                 def _():
-                    remote(src, src, lat_up, (z,), (z,), me + nx, tp).start()
+                    hop(src, 1, z, me + nx).start()
 
                 lat_share(z)
 
@@ -419,11 +428,11 @@
             def _():
                 z = my_z + d
                 src = g_lat.at[own_lat, z]
-                come(src, lat_dn, (z,))
+                hop(src, 2, z, me, mate).wait_recv()
 
                 @pl.when(my_z > 0)
                 def _():
-                    remote(src, src, lat_dn, (z,), (z,), me - nx, tp).start()
+                    hop(src, 2, z, me - nx).start()
 
                 lat_share(z)
 
@@ -450,11 +459,11 @@
 
             @pl.when(jnp.logical_and(my_z >= z, my_z + 1 < nz))
             def _():
-                remote(block, block, lat_up, (z,), (z,), me, mate).wait_send()
+                hop(block, 1, z, me, mate).wait_send()
 
             @pl.when(jnp.logical_and(my_z <= z, my_z > 0))
             def _():
-                remote(block, block, lat_dn, (z,), (z,), me, mate).wait_send()
+                hop(block, 2, z, me, mate).wait_send()
 
             remote(block, block, lat_c, (0, z), (0, z), me, mate).wait_send()
             if nx > 1:
@@ -776,9 +785,9 @@
             if d > 2:
                 scoped("expand%d" % (d - 2), around, d - 2, expand)
     each("combine", combine, 0)
+    scoped("give_back%d" % final, give_back, final)
     if nz > 1:
         scoped("expand%d" % last, around, last, expand)
-    scoped("give_back%d" % final, give_back, final)
     for p in range(parts):
         scoped("attend%d" % p, attend, p)
         att_send(p)
@@ -887,8 +896,7 @@
             pltpu.VMEM((row_count, out_proj.shape[1]), bf16),
             pltpu.VMEM((row_count, columns), bf16),
             pltpu.SemaphoreType.DMA((15,)),
-            dma(nz),
-            dma(nz),
+            pltpu.SemaphoreType.DMA((3, nz)),
             dma(nz),
             dma(nx, nz),
             dma(n_ep),

time: 63.4 us -> 63.3 us (level)
  no operation moved by 1% of the time
where the time goes in v5:
time: 63.3 us; the launch traced here: 63.1 us
  Pallas kernels  61.1 us (97%)
  local copies, waits for them, and re-layouts  1.41 us (2%)
  between operations  0.64 us (1%)
    pallas_call x1, Pallas kernels, local(): pl.pallas_call(functools.partial(fused, n_ep, n_tp, heads, (PLAIN_HEAD_DI...  61.1 us
    unnamed x2, local copies, waits for them, and re-layouts  1.41 us

profile of v5, /device:TPU:0, one launch (start us, length us, event | category | flops | bytes accessed | tf_op | source)
XLA Modules:
  0.0 63.1 jit_solution(2867162560923411793)
XLA Ops:
  0.6 61.1 %fused.1 = (bf16[256,512]{1,0:T(8,128)(2,1)S(1)}, bf16[256,512]{1,0:T(8,128)(2,1)S(1)}) custom-call(s32[2,256]{1,0:T(2,128)} %bitcast.13, f32[2,256]{1,0:T(2,128)} %bitcast.14, f32[1,2048]{1,0:T(1,128)} %bitcast.12, f32[1,512]{1,0:T(1,128)} %bitcast.15, bf16[32,256]{1,0:T(8,128)(2,1)} %bitcast.11, bf16[256,2048]{1,0:T(8,128)(2,1)} %moe_hbm.1, ...), custom_call_target="tpu_custom_call" | custom-call | tf_op jit(solution)/shard_map/fused/pallas_call | solution.py:855
  61.7 0.7 %copy.17 = bf16[256,512]{1,0:T(8,128)(2,1)} copy(bf16[256,512]{1,0:T(8,128)(2,1)S(1)} %get-tuple-element.2) | data formatting | bytes 524288
  62.4 0.7 %copy.18 = bf16[256,512]{1,0:T(8,128)(2,1)} copy(bf16[256,512]{1,0:T(8,128)(2,1)S(1)} %get-tuple-element.3) | data formatting | bytes 524288
